TPU v7x, 128 devices: a whole 4x4x4 slice. The times are simulated.
128 devices in a mesh: sp: 16 (over z, y), dp: 8 (over x, core).
Axes of the slice: x: 4, y: 4, z: 4, core: 2. Of those that a mesh axis runs over, the one named last changes fastest.
Arguments:
- queries: bfloat16 [8, 2048, 2048], P('dp', 'sp'), may hold values from -40 to 40
- keys: bfloat16 [8, 2048, 512], P('dp', 'sp'), may hold values from -8 to 8
- values: bfloat16 [8, 2048, 512], P('dp', 'sp'), may hold values from -6 to 6
- lambdas: float32 [16], replicated, may hold values from 0.3 to 0.8
- value_gain: float32 [128], replicated, may hold values from 0.1 to 1.9
- out_weight: bfloat16 [2048, 4096], P(None, ('sp', 'dp')), may hold values from -0.125 to 0.125
Outputs:
- mixed: bfloat16 [8, 2048, 4096], P('dp', 'sp')
All inputs are finite; a program needn't handle non-finite values.
Results may differ from a plain program's by a relative error of at most 0.0087.
Values may be sent and summed in bfloat16 or wider, within the bound.
A program may use at most 128 MiB of HBM per device.

v0:
```python
import jax
import jax.numpy as jnp
from jax import lax
from jax.sharding import PartitionSpec as P

HEADS = 16
KV_HEADS = 4
HEAD_DIM = 64
VALUE_DIM = 128


rope_base = 500000.0
output_scale = 0.8
norm_eps = 1e-05


def rotate(parts, positions):
    width = parts.shape[-1]
    half = width // 2
    freqs = rope_base ** (-jnp.arange(0, width, 2, dtype=jnp.float32) / width)
    angles = positions[:, None] * freqs[None, :]
    shape = (angles.shape[0],) + (1,) * (parts.ndim - 2) + (half,)
    cosine = jnp.cos(angles).reshape(shape)
    sine = jnp.sin(angles).reshape(shape)
    first = parts[..., :half]
    second = parts[..., half:]
    return jnp.concatenate([first * cosine - second * sine, second * cosine + first * sine], -1)


def attend(query_rot, key_rot, value_whole, lambda_heads, value_gain):
    seqlen = key_rot.shape[0]
    block_rows = min(512, seqlen)
    count = seqlen // block_rows
    score_scale = query_rot.shape[-1] ** (-0.5)
    outputs = []
    for block_index in range(count):
        start = block_index * block_rows
        reach = start + block_rows
        query_block = query_rot[start:reach]
        key_part = key_rot[:reach]
        value_part = value_whole[:reach]
        scores = (
            jnp.einsum("qhmd,kmd->hmqk", query_block, key_part, preferred_element_type=jnp.float32)
            * score_scale
        )
        allowed = jnp.arange(reach)[None, :] <= (start + jnp.arange(block_rows))[:, None]
        scores = jnp.where(allowed[None, None], scores, -jnp.inf)
        row_top = jnp.max(scores, -1, keepdims=True)
        raised = jnp.exp(scores - row_top)
        maps = raised / jnp.sum(raised, -1, keepdims=True)
        weights = (maps[:, 0] - lambda_heads[:, None, None] * maps[:, 1]).astype(jnp.bfloat16)
        outputs.append(
            jnp.einsum("hqk,ke->qhe", weights, value_part, preferred_element_type=jnp.float32)
        )
    head_values = jnp.concatenate(outputs, 0)
    squares = jnp.mean(head_values * head_values, -1, keepdims=True)
    normed = head_values * lax.rsqrt(squares + norm_eps) * value_gain * output_scale
    return normed.astype(jnp.bfloat16)


def shards(queries, keys, values, lambdas, value_gain, out_weight):
    tok_rows = queries.shape[1]
    sp_count = lax.axis_size("sp")
    group_size = sp_count // KV_HEADS
    per_device = HEADS // sp_count
    query_split = queries[0].reshape(tok_rows, HEADS, 2 * HEAD_DIM)
    key_split = keys[0].reshape(tok_rows, KV_HEADS, 2 * HEAD_DIM)
    value_split = values[0].reshape(tok_rows, KV_HEADS, VALUE_DIM)
    key_copies = jnp.repeat(key_split, group_size, axis=1)
    value_copies = jnp.repeat(value_split, group_size, axis=1)
    query_heads, key_heads, value_heads = (
        lax.all_to_all(query_split, "sp", split_axis=1, concat_axis=0, tiled=True),
        lax.all_to_all(key_copies, "sp", split_axis=1, concat_axis=0, tiled=True),
        lax.all_to_all(value_copies, "sp", split_axis=1, concat_axis=0, tiled=True),
    )
    key_whole = key_heads[:, 0]
    value_whole = value_heads[:, 0]
    seqlen = query_heads.shape[0]
    positions = jnp.arange(seqlen, dtype=jnp.float32)
    query_rot = rotate(
        query_heads.reshape(seqlen, per_device, 2, HEAD_DIM).astype(jnp.float32), positions
    ).astype(jnp.bfloat16)
    key_rot = rotate(key_whole.reshape(seqlen, 2, HEAD_DIM).astype(jnp.float32), positions).astype(
        jnp.bfloat16
    )
    lambda_heads = lax.dynamic_slice_in_dim(
        lambdas, lax.axis_index("sp") * per_device, per_device, 0
    )
    head_out = attend(query_rot, key_rot, value_whole, lambda_heads, value_gain)
    heads_local = lax.all_to_all(
        head_out.reshape(seqlen, per_device * VALUE_DIM),
        "sp",
        split_axis=0,
        concat_axis=1,
        tiled=True,
    )
    mixed = jnp.dot(
        heads_local,
        lax.all_gather(out_weight, ("sp", "dp"), axis=1, tiled=True),
        preferred_element_type=jnp.float32,
    ).astype(jnp.bfloat16)
    return mixed[None]


def solution(mesh):
    return jax.shard_map(
        shards,
        mesh=mesh,
        in_specs=(
            P("dp", "sp", None),
            P("dp", "sp", None),
            P("dp", "sp", None),
            P(),
            P(),
            P(None, ("sp", "dp")),
        ),
        out_specs=P("dp", "sp", None),
        check_vma=False,
    )
```

profile of v0, /device:TPU:2, one launch (start us, length us, event | category | flops | bytes accessed | tf_op | source)
XLA Modules:
  0.0 124.7 jit_solution(13890816963404634204)
XLA Ops:
  6.5 0.0 copy-start.4
  6.5 0.0 all-gather.2.cloned.1.call-start
  6.5 0.7 all-gather.2.cloned.1.call-update
  7.3 1.0 copy.19
  8.3 0.9 broadcast_in_dim.51
  9.2 8.0 %all-to-all-start = ((bf16[128,16,128]{0,2,1:T(8,128)(2,1)}), bf16[128,16,128]{0,2,1:T(8,128)(2,1)S(1)}, u32[]{:S(2)}, u32[]{:S(2)}) async-start(bf16[128,16,128]{0,2,1:T(8,128)(2,1)} %bitcast.1), calls=%async_computation | async-start | bytes 1048576 | tf_op jit(solution)/shard_map/all_to_all | solution.py:73
  17.3 0.8 iota_compare_fusion.3
  18.0 1.8 %fusion.42 = (f32[2048,32]{0,1:T(8,128)}, f32[2048,32]{0,1:T(8,128)}) fusion(f32[32]{0:T(128)S(1)} %multiply_power_fusion), kind=kLoop, calls=%fused_computation.74 | loop fusion | flops 65536 | bytes 524416 | tf_op jit(solution)/shard_map/cos | solution.py:23
  19.9 0.9 reshape_squeeze.12
  20.8 0.6 iota_compare_fusion.1
  21.4 7.4 %all-to-all-done = bf16[128,16,128]{0,2,1:T(8,128)(2,1)S(1)} async-done(((bf16[128,16,128]{0,2,1:T(8,128)(2,1)}), bf16[128,16,128]{0,2,1:T(8,128)(2,1)S(1)}, u32[]{:S(2)}, u32[]{:S(2)}) %all-to-all-start) | async-done | bytes 524320 | tf_op jit(solution)/shard_map/all_to_all | solution.py:73
  28.8 0.9 broadcast_in_dim.53
  29.7 3.6 %all-to-all-start.2 = ((bf16[128,16,128]{2,0,1:T(8,128)(2,1)}), bf16[128,16,128]{2,0,1:T(8,128)(2,1)S(1)}, u32[]{:S(2)}, u32[]{:S(2)}) async-start(bf16[128,16,128]{2,0,1:T(8,128)(2,1)} %bitcast.12), calls=%async_computation.2 | async-start | bytes 1048576 | tf_op jit(solution)/shard_map/all_to_all | solution.py:74
  33.3 0.0 copy-done.4
  33.3 1.0 copy.15
  34.3 0.0 copy-done.8
  34.3 0.6 dynamic_slice.3
  34.9 0.8 iota_compare_fusion
  35.7 8.0 %all-to-all-done.2 = bf16[128,16,128]{2,0,1:T(8,128)(2,1)S(1)} async-done(((bf16[128,16,128]{2,0,1:T(8,128)(2,1)}), bf16[128,16,128]{2,0,1:T(8,128)(2,1)S(1)}, u32[]{:S(2)}, u32[]{:S(2)}) %all-to-all-start.2) | async-done | bytes 524320 | tf_op jit(solution)/shard_map/all_to_all | solution.py:74
  43.7 4.4 %all-to-all-start.1 = ((bf16[128,16,128]{0,2,1:T(8,128)(2,1)}), bf16[128,16,128]{0,2,1:T(8,128)(2,1)}, u32[]{:S(2)}, u32[]{:S(2)}) async-start(bf16[128,16,128]{0,2,1:T(8,128)(2,1)} %bitcast.4), calls=%async_computation.1 | async-start | bytes 1048576 | tf_op jit(solution)/shard_map/all_to_all | solution.py:72
  48.1 0.4 iota_compare_fusion.2
  48.5 0.7 slice.115
  49.2 0.8 slice.122
  50.0 0.1 convert_bitcast_fusion.1
  50.1 0.0 copy-done
  50.1 1.6 %copy.14 = f32[16,128,1,128]{1,0,3,2:T(8,128)} copy(f32[16,128,1,128]{1,3,0,2:T(8,128)S(1)} %convert_bitcast_fusion.1) | data formatting | bytes 2097152 | tf_op jit(solution)/shard_map/convert_element_type | solution.py:83
  51.7 1.4 %reshape.478 = f32[2048,2,64]{0,2,1:T(8,128)S(1)} reshape(f32[16,128,1,128]{1,0,3,2:T(8,128)} %copy.14) | data formatting | bytes 2097152 | tf_op jit(solution)/shard_map/convert_element_type | solution.py:83
  53.1 8.3 %all-to-all-done.1 = bf16[128,16,128]{0,2,1:T(8,128)(2,1)} async-done(((bf16[128,16,128]{0,2,1:T(8,128)(2,1)}), bf16[128,16,128]{0,2,1:T(8,128)(2,1)}, u32[]{:S(2)}, u32[]{:S(2)}) %all-to-all-start.1) | async-done | bytes 524320 | tf_op jit(solution)/shard_map/all_to_all | solution.py:72
  61.5 1.1 convert_bitcast_fusion
  62.6 1.6 %copy.16 = f32[16,128,1,128]{1,0,3,2:T(8,128)} copy(f32[16,128,1,128]{1,3,0,2:T(8,128)S(1)} %convert_bitcast_fusion) | data formatting | bytes 2097152 | tf_op jit(solution)/shard_map/convert_element_type | solution.py:81
  64.2 2.4 %reshape.479 = f32[2048,1,2,64]{0,3,2,1:T(8,128)} reshape(f32[16,128,1,128]{1,0,3,2:T(8,128)} %copy.16) | data formatting | bytes 2097152 | tf_op jit(solution)/shard_map/convert_element_type | solution.py:81
  66.6 1.2 subtract_convert_fusion.1
  67.8 1.5 %subtract_convert_fusion = (bf16[2048,1,2,32]{0,3,2,1:T(8,128)(2,1)S(1)}, bf16[2048,1,2,32]{0,3,2,1:T(8,128)(2,1)S(1)}) fusion(f32[2048,1,2,64]{0,3,2,1:T(8,128)} %reshape.479, f32[2048,32]{0,1:T(8,128)} %get-tuple-element.10, f32[2048,32]{0,1:T(8,128)} %get-tuple-element.9), kind=kLoop, calls=%fused_computation.65 | loop fusion | flops 1048576 | bytes 2097152 | tf_op jit(solution)/shard_map/convert.6
  69.3 0.0 copy-done.2
  69.3 0.6 fusion.62
  69.9 0.3 fusion.20
  70.2 0.3 fusion.19
  70.5 1.0 fusion.32
  71.6 1.1 fusion.11
  72.6 1.0 fusion.10
  73.6 1.0 fusion.9
  74.6 0.0 copy-done.6
  74.6 1.2 fusion.28
  75.8 1.5 %fusion.5 = (f32[2,512]{1,0:T(2,128)S(1)}, f32[2,1536,512]{2,1,0:T(8,128)S(1)}) fusion(pred[512,1536]{0,1:T(8,128)(4,1)S(1)} %iota_compare_fusion.1, bf16[2048,1,2,32]{0,3,2,1:T(8,128)(2,1)S(1)} %get-tuple-element.5, bf16[2048,1,2,32]{0,3,2,1:T(8,128)(2,1)S(1)} %get-tuple-element.6, bf16[2048,2,32]{0,2,1:T(8,128)(2,1)S(1)} %get-tuple-element.7, ...), kind=kOutput, calls=%fused_computation.10 | convolution fusion | flops 207092736 | bytes 8130560 | tf_op jit(solution)/shard_map/qhmd,kmd->hmqk/dot_general | solution.py:43
  77.3 1.5 %fusion.4 = f32[2,512]{1,0:T(2,128)S(1)} fusion(f32[2,1536,512]{2,1,0:T(8,128)S(1)} %get-tuple-element.14, f32[2,512]{1,0:T(2,128)S(1)} %get-tuple-element.13, pred[512,1536]{0,1:T(8,128)(4,1)S(1)} %iota_compare_fusion.1), kind=kLoop, calls=%fused_computation.8 | loop fusion | flops 6290432 | bytes 7086080 | tf_op jit(solution)/shard_map/reduce_sum | solution.py:50
  78.8 1.7 %fusion.3 = f32[1,2,512,1536]{2,3,1,0:T(8,128)S(1)} fusion(f32[2,1536,512]{2,1,0:T(8,128)S(1)} %get-tuple-element.14, f32[2,512]{1,0:T(2,128)S(1)} %fusion.4, f32[2,512]{1,0:T(2,128)S(1)} %get-tuple-element.13, pred[512,1536]{0,1:T(8,128)(4,1)S(1)} %iota_compare_fusion.1), kind=kLoop, calls=%fused_computation.7 | loop fusion | flops 6291456 | bytes 13377536 | tf_op jit(solution)/shard_map/div | solution.py:50
  80.5 0.0 copy-done.5
  80.5 1.5 %fusion.22 = f32[512,128]{1,0:T(8,128)S(1)} fusion(bf16[1536,128]{1,0:T(8,128)(2,1)S(1)} %bitcast.127, f32[1,2,512,1536]{2,3,1,0:T(8,128)S(1)} %fusion.3, f32[]{:T(128)} %bitcast.10), kind=kOutput, calls=%fused_computation.36 | convolution fusion | flops 203685888 | bytes 6946820 | tf_op jit(solution)/shard_map/hqk,ke->qhe/dot_general | solution.py:53
  82.0 1.9 %fusion.2 = (f32[2,512]{1,0:T(2,128)S(1)}, f32[2,2048,512]{2,1,0:T(8,128)S(1)}) fusion(pred[512,2048]{0,1:T(8,128)(4,1)S(1)} %iota_compare_fusion, bf16[2048,1,2,32]{0,3,2,1:T(8,128)(2,1)S(1)} %get-tuple-element.6, bf16[2048,1,2,32]{0,3,2,1:T(8,128)(2,1)S(1)} %get-tuple-element.5, bf16[2048,2,32]{0,2,1:T(8,128)(2,1)S(1)} %get-tuple-element.8, ...), kind=kOutput, calls=%fused_computation.4 | convolution fusion | flops 276036608 | bytes 10489856 | tf_op jit(solution)/shard_map/qhmd,kmd->hmqk/dot_general | solution.py:43
  83.9 2.0 %fusion.1 = f32[2,512]{1,0:T(2,128)S(1)} fusion(f32[2,2048,512]{2,1,0:T(8,128)S(1)} %get-tuple-element.12, f32[2,512]{1,0:T(2,128)S(1)} %get-tuple-element.11, pred[512,2048]{0,1:T(8,128)(4,1)S(1)} %iota_compare_fusion), kind=kLoop, calls=%fused_computation.3 | loop fusion | flops 8387584 | bytes 9445376 | tf_op jit(solution)/shard_map/reduce_sum | solution.py:50
  85.9 0.0 copy-start.1
  86.0 2.0 %fusion = f32[1,2,512,2048]{2,3,1,0:T(8,128)S(1)} fusion(f32[2,2048,512]{2,1,0:T(8,128)S(1)} %get-tuple-element.12, f32[2,512]{1,0:T(2,128)S(1)} %fusion.1, f32[2,512]{1,0:T(2,128)S(1)} %get-tuple-element.11, pred[512,2048]{0,1:T(8,128)(4,1)S(1)} %iota_compare_fusion), kind=kLoop, calls=%fused_computation.2 | loop fusion | flops 8388608 | bytes 17833984 | tf_op jit(solution)/shard_map/div | solution.py:50
  87.9 0.0 copy-done.1
  87.9 0.0 copy-start.7
  88.0 1.7 %fusion.17 = f32[512,128]{1,0:T(8,128)S(1)} fusion(bf16[2048,128]{1,0:T(8,128)(2,1)S(1)} %bitcast.119, f32[1,2,512,2048]{2,3,1,0:T(8,128)S(1)} %fusion, f32[]{:T(128)} %bitcast.10), kind=kOutput, calls=%fused_computation.32 | convolution fusion | flops 271581184 | bytes 9175044 | tf_op jit(solution)/shard_map/hqk,ke->qhe/dot_general | solution.py:53
  89.7 0.0 copy-start.3
  89.7 0.1 pad_maximum_fusion
  89.8 0.6 copy-done.3
  90.4 0.3 copy.18
  90.7 1.3 %fusion.27 = f32[2048]{0:T(1024)S(1)} fusion(f32[512,1,128]{2,0,1:T(8,128)} %bitcast.124, f32[512,1,128]{2,0,1:T(8,128)S(1)} %bitcast.123, f32[512,1,128]{2,0,1:T(8,128)S(1)} %bitcast.122, f32[512,1,128]{2,0,1:T(8,128)S(1)} %bitcast.120), kind=kLoop, calls=%fused_computation.43 | loop fusion | flops 1308672 | bytes 1056768 | tf_op jit(solution)/shard_map/reduce_sum | solution.py:56
  92.0 0.0 copy-done.7
  92.0 0.2 multiply_convert_fusion
  92.3 13.1 %all_to_all.49 = bf16[16,128,128]{1,2,0:T(8,128)(2,1)S(1)} all-to-all(bf16[16,128,128]{1,2,0:T(8,128)(2,1)S(1)} %multiply_convert_fusion), channel_id=1, replica_groups=mesh['sp'=16,'dp'=8] {'sp'}, dimensions={0} | all-to-all | bytes 1048576 | tf_op jit(solution)/shard_map/all_to_all | solution.py:90
  105.3 12.5 %fusion.6 = bf16[1,128,4096]{2,1,0:T(8,128)(2,1)} fusion(bf16[128,2048]{0,1:T(8,128)(2,1)S(1)} %bitcast.121, bf16[2048,4096]{0,1:T(8,128)(2,1)} %all-gather.2.cloned.1.call-done), kind=kOutput, calls=%fused_computation.11 | convolution fusion | flops 2148007936 | bytes 18350080 | tf_op jit(solution)/shard_map/dot_general | solution.py:97
  (13 shorter events, 0.1 us)
Async XLA Ops:
  6.5 26.8 %copy-start.4 = (bf16[1,128,2048]{2,1,0:T(8,128)(2,1)S(1)}, bf16[1,128,2048]{2,1,0:T(8,128)(2,1)}, u32[]{:S(2)}) copy-start(bf16[1,128,2048]{2,1,0:T(8,128)(2,1)} %param.6) | copy-start | bytes 1572868
  6.5 27.8 %copy-start.8 = (f32[16]{0:T(128)S(1)}, f32[16]{0:T(128)}, u32[]{:S(2)}) copy-start(f32[16]{0:T(128)} %param.9) | copy-start | bytes 196
  6.5 98.8 %all-gather.2.cloned.1.call-start = ((), (), s32[]{:S(2)}) async-start(), calls=%async_computation.4 | async-start | bytes 16908288 | tf_op jit(solution)/shard_map/all_gather | solution.py:99
  9.2 19.6 %all-to-all-start = ((bf16[128,16,128]{0,2,1:T(8,128)(2,1)}), bf16[128,16,128]{0,2,1:T(8,128)(2,1)S(1)}, u32[]{:S(2)}, u32[]{:S(2)}) async-start(bf16[128,16,128]{0,2,1:T(8,128)(2,1)} %bitcast.1), calls=%async_computation | async-start | bytes 1048576 | tf_op jit(solution)/shard_map/all_to_all | solution.py:73
  29.7 14.0 %all-to-all-start.2 = ((bf16[128,16,128]{2,0,1:T(8,128)(2,1)}), bf16[128,16,128]{2,0,1:T(8,128)(2,1)S(1)}, u32[]{:S(2)}, u32[]{:S(2)}) async-start(bf16[128,16,128]{2,0,1:T(8,128)(2,1)} %bitcast.12), calls=%async_computation.2 | async-start | bytes 1048576 | tf_op jit(solution)/shard_map/all_to_all | solution.py:74
  43.7 6.4 %copy-start = (bf16[128,16,128]{2,0,1:T(8,128)(2,1)}, bf16[128,16,128]{2,0,1:T(8,128)(2,1)S(1)}, u32[]{:S(2)}) copy-start(bf16[128,16,128]{2,0,1:T(8,128)(2,1)S(1)} %all-to-all-done.2) | copy-start | bytes 1572868
  43.7 17.8 %all-to-all-start.1 = ((bf16[128,16,128]{0,2,1:T(8,128)(2,1)}), bf16[128,16,128]{0,2,1:T(8,128)(2,1)}, u32[]{:S(2)}, u32[]{:S(2)}) async-start(bf16[128,16,128]{0,2,1:T(8,128)(2,1)} %bitcast.4), calls=%async_computation.1 | async-start | bytes 1048576 | tf_op jit(solution)/shard_map/all_to_all | solution.py:72
  66.6 2.7 %copy-start.2 = (pred[512,512]{0,1:T(8,128)(4,1)S(1)}, pred[512,512]{0,1:T(8,128)(4,1)}, u32[]{:S(2)}) copy-start(pred[512,512]{0,1:T(8,128)(4,1)} %iota_compare_fusion.3) | copy-start | bytes 786436
  73.6 1.0 copy-start.6
  78.8 1.7 %copy-start.5 = (bf16[12,128,1,128]{3,1,0,2:T(8,128)(2,1)S(1)}, bf16[12,128,1,128]{3,1,0,2:T(8,128)(2,1)}, u32[]{:S(2)}) copy-start(bf16[12,128,1,128]{3,1,0,2:T(8,128)(2,1)} %slice.122) | copy-start | bytes 1179652
  85.9 2.0 %copy-start.1 = (bf16[128,16,128]{2,0,1:T(8,128)(2,1)S(1)}, bf16[128,16,128]{2,0,1:T(8,128)(2,1)}, u32[]{:S(2)}) copy-start(bf16[128,16,128]{2,0,1:T(8,128)(2,1)} %copy-done) | copy-start | bytes 1572868
  87.9 4.1 %copy-start.7 = (f32[128]{0:T(128)S(1)}, f32[128]{0:T(128)}, u32[]{:S(2)}) copy-start(f32[128]{0:T(128)} %param.10) | copy-start | bytes 1540
  89.7 0.7 copy-start.3
Sparse Core Ops, SparseCore 0:
  10.5 86.9 all-gather.1
where the time goes:
time: 125 us
  waiting for transfers between devices  24.4 us (20%)
  matrix products  23 us (18%)
  other arithmetic  19.6 us (16%)
  starting transfers between devices  16 us (13%)
  local copies, waits for them, and re-layouts  14.8 us (12%)
  between operations  13.7 us (11%)
  blocking collectives  13.1 us (10%)
    all_to_all x1, blocking collectives, shards(): lax.all_to_all(head_out.reshape(seqlen, per_device * VALUE_DIM), 'sp', sp...  13.1 us
    dot_general x1, matrix products, shards(): jnp.dot(heads_local, lax.all_gather(out_weight, ('sp', 'dp'), axis=1, til...  12.5 us
    all_to_all x1, waiting for transfers between devices, shards(): lax.all_to_all(query_split, 'sp', split_axis=1, concat_axis=0, tiled=True)  8.35 us
    all_to_all x1, starting transfers between devices, shards(): lax.all_to_all(key_copies, 'sp', split_axis=1, concat_axis=0, tiled=True)  8.05 us
    all_to_all x1, waiting for transfers between devices, shards(): lax.all_to_all(value_copies, 'sp', split_axis=1, concat_axis=0, tiled=True)  7.97 us
    all_to_all x1, waiting for transfers between devices, shards(): lax.all_to_all(key_copies, 'sp', split_axis=1, concat_axis=0, tiled=True)  7.36 us
    dot_general x4, matrix products, attend(): jnp.einsum('hqk,ke->qhe', weights, value_part, preferred_element_type=jnp...  5.45 us
    dot_general x4, matrix products, attend(): jnp.einsum('qhmd,kmd->hmqk', query_block, key_part, preferred_element_typ...  5.07 us
  transfers between devices with their start and end apart: 4, of which 3 were waited for; matrix products, arithmetic and copies ran while one was open for 36% of the time, Pallas kernels for 0%

commit v1 on v0

v1 whole, which is shorter than its diff:
```python
import functools

import jax
import jax.numpy as jnp
import numpy as np
from jax import lax
from jax.experimental import pallas as pl
from jax.experimental.pallas import tpu as pltpu
from jax.sharding import PartitionSpec as P

HEADS = 16
KV_HEADS = 4
HEAD_DIM = 64
VALUE_DIM = 128
D = 4096
SEQLEN = 2048
ROWS = 128
GROUP = HEADS // KV_HEADS
KT = 256
ROPE_BASE = 500000.0
OUTPUT_SCALE = 0.8
NORM_EPS = 1e-05
MESH = pl.DeviceIdType.MESH

COLOURS = (
    (("y", "z", "x"), 0, 1024),
    (("x", "z", "y"), 1024, 768),
    (("x", "y", "z"), 1792, 256),
)


def rotation_tables():
    f32 = np.float32
    freqs = (f32(ROPE_BASE) ** (-np.arange(0, HEAD_DIM, 2, dtype=f32) / f32(HEAD_DIM))).astype(f32)
    lanes = np.tile(freqs.astype(np.float64), 4)
    inner = np.arange(ROWS)[:, None] * lanes[None]
    outer = (np.arange(SEQLEN // ROWS) * ROWS)[:, None] * lanes[None]
    inner = np.stack([np.cos(inner), np.sin(inner)]).astype(f32)
    outer = np.stack([np.cos(outer), np.sin(outer)], 1).astype(f32)
    return inner, outer


def kernel(
    lam_ref, q_hbm, k_hbm, v_hbm, gain_ref, inner_ref, outer_ref, w_hbm,
    out_ref,
    q_in, k_in, v_in, kvst, kv, qst, qin, q2, sbuf, acc, wbuf, hst, acts, oown, opart, oin,
    in_sem, kvz_s, kvz_r, kvy_s, kvy_r, qz_s, qz_r, w_s, w_r, oz_s, oz_r, af_s, af_r, oo_s, oo_r,
):
    f32, bf16 = jnp.float32, jnp.bfloat16
    sp, dp = lax.axis_index("sp"), lax.axis_index("dp")
    me = {"z": sp // 4, "y": lax.rem(sp, 4), "x": dp // 2}
    core = lax.rem(dp, 2)

    def at(pos):
        return (pos["z"] * 4 + pos["y"], pos["x"] * 2 + core)

    def shift(dim, off):
        return {**me, dim: lax.rem(me[dim] + off + 4, 4)}

    partner = (sp, me["x"] * 2 + 1 - core)
    pending = []

    def send(src, dst, s_sem, r_sem, dev):
        copy = pltpu.make_async_remote_copy(
            src_ref=src, dst_ref=dst, send_sem=s_sem, recv_sem=r_sem, device_id=dev, device_id_type=MESH
        )
        copy.start()
        pending.append(copy)

    def arrived(dst, s_sem, r_sem):
        pltpu.make_async_remote_copy(
            src_ref=dst, dst_ref=dst, send_sem=s_sem, recv_sem=r_sem, device_id=partner, device_id_type=MESH
        ).wait_recv()

    c_k = pltpu.make_async_copy(k_hbm, k_in, in_sem.at[0])
    c_v = pltpu.make_async_copy(v_hbm, v_in, in_sem.at[1])
    c_w = pltpu.make_async_copy(w_hbm, wbuf.at[me["z"], me["y"], me["x"]], in_sem.at[2])
    c_q = pltpu.make_async_copy(q_hbm, q_in, in_sem.at[3])
    for c in (c_k, c_v, c_w, c_q):
        c.start()

    barrier = pltpu.get_barrier_semaphore()
    peers = [at(shift("z", o)) for o in (1, 2, 3)] + [at(shift("y", o)) for o in (1, 3)]
    peers += [at(shift("x", o)) for o in (1, 3)] + [partner]
    for dev in peers:
        pl.semaphore_signal(barrier, inc=1, device_id=dev, device_id_type=MESH)

    ci, si = inner_ref[0], inner_ref[1]
    co, so = outer_ref[sp, 0:1, :], outer_ref[sp, 1:2, :]
    cosine = co * ci - so * si
    sine = so * ci + co * si
    row = lax.broadcasted_iota(jnp.int32, (128, 128), 0)
    col = lax.broadcasted_iota(jnp.int32, (128, 128), 1)
    low = lax.rem(col, 64) < 32
    swap = jnp.where(
        low & (row == col + 32), -1.0, jnp.where(jnp.logical_not(low) & (row == col - 32), 1.0, 0.0)
    ).astype(bf16)

    def rotate(part):
        turned = jnp.dot(part, swap, preferred_element_type=f32)
        return (part.astype(f32) * cosine + turned * sine).astype(bf16)

    c_k.wait()
    c_v.wait()
    for g in range(KV_HEADS):
        cols = slice(g * 128, (g + 1) * 128)
        kvst[g, 0] = rotate(k_in[:, cols])
        kvst[g, 1] = v_in[:, cols].astype(f32).T.astype(bf16)
    kv[sp, 0] = kvst[me["z"], 0]
    kv[sp, 1] = kvst[me["z"], 1]
    pl.semaphore_wait(barrier, len(peers))

    for o in (1, 3, 2):
        pos = shift("z", o)
        send(kvst.at[pos["z"]], kv.at[sp], kvz_s.at[o - 1], kvz_r.at[o - 1], at(pos))

    def kv_block(rel, off):
        return lax.rem(me["z"] + rel, 4) * 4 + lax.rem(me["y"] + off + 4, 4)

    def kvy_start(rel):
        view = kvst.at[me["z"]] if rel == 0 else kv.at[kv_block(rel, 0)]
        dst = kv.at[kv_block(rel, 0)]
        for slot, off in ((0, 1), (1, -1)):
            send(view, dst, kvy_s.at[rel * 4 + slot], kvy_r.at[rel * 4 + slot], at(shift("y", off)))

    def kvy_forward(rel):
        for slot, off in ((0, -1), (1, 1)):
            view = kv.at[kv_block(rel, off)]
            arrived(view, kvy_s.at[rel * 4 + slot], kvy_r.at[rel * 4 + slot])
            half = kv.at[kv_block(rel, off), slot]
            n = rel * 4 + slot + 2
            send(half, half, kvy_s.at[n], kvy_r.at[n], at(shift("y", -off)))

    def kvy_finish(rel):
        for slot in (0, 1):
            n = rel * 4 + slot + 2
            arrived(kv.at[kv_block(rel, 2), slot], kvy_s.at[n], kvy_r.at[n])

    def kvz_wait(rel):
        o = 4 - rel
        arrived(kv.at[kv_block(rel, 0)], kvz_s.at[o - 1], kvz_r.at[o - 1])

    kvy_start(0)

    def wview(ci_, phase, b1=None, b2=None, b3=None, half=None):
        order, k0, kn = COLOURS[ci_]
        sel = dict(me)
        rows = slice(None)
        if phase == 1:
            sel[order[0]] = b1
            if half is not None:
                rows = pl.ds(16 * half, 16)
        else:
            sel[order[0]] = slice(None) if half is None else pl.ds(2 * half, 2)
            sel[order[1]] = b2
            if phase == 3:
                sel[order[2]] = b3
        return wbuf.at[sel["z"], sel["y"], sel["x"], rows, pl.ds(k0, kn)]

    class Ring:
        def __init__(self, ci_, phase, rel=0):
            self.ci, self.phase, self.rel = ci_, phase, rel
            self.dim = COLOURS[ci_][0][phase - 1]
            self.base = ci_ * 24 + (phase - 1 + rel if phase == 3 else phase - 1) * 4

        def view(self, off, half=None):
            spot = lax.rem(me[self.dim] + off + 4, 4)
            if self.phase == 1:
                return wview(self.ci, 1, b1=spot, half=half)
            if self.phase == 2:
                return wview(self.ci, 2, b2=spot, half=half)
            other = COLOURS[self.ci][0][1]
            return wview(self.ci, 3, b2=lax.rem(me[other] + self.rel, 4), b3=spot, half=half)

        def start(self):
            view = self.view(0)
            for slot, off in ((0, 1), (1, -1)):
                n = self.base + slot
                send(view, view, w_s.at[n], w_r.at[n], at(shift(self.dim, off)))

        def forward(self, slot):
            off = (-1, 1)[slot]
            n = self.base + slot
            arrived(self.view(off), w_s.at[n], w_r.at[n])
            half = self.view(off, slot)
            send(half, half, w_s.at[n + 2], w_r.at[n + 2], at(shift(self.dim, -off)))

        def finish(self):
            for slot in (0, 1):
                n = self.base + slot + 2
                arrived(self.view(2, slot), w_s.at[n], w_r.at[n])

    p1 = [Ring(c, 1) for c in range(3)]
    p2 = [Ring(c, 2) for c in range(3)]
    p3 = [[Ring(c, 3, r) for r in range(4)] for c in range(3)]

    c_w.wait()
    for c in range(3):
        p1[c].start()

    c_q.wait()
    for g in range(KV_HEADS):
        for h in range(GROUP):
            a = (g * GROUP + h) * 128
            qst[g, :, h * 128:(h + 1) * 128] = rotate(q_in[:, a:a + 128])
    for o in (1, 3, 2):
        pos = shift("z", o)
        send(qst.at[pos["z"]], qin.at[me["z"]], qz_s.at[o - 1], qz_r.at[o - 1], at(pos))
    qin[me["z"]] = qst[me["z"]]

    kvz_wait(3)
    kvy_start(3)
    kvz_wait(1)
    kvy_start(1)
    kvy_forward(0)
    for c in range(3):
        p1[c].forward(0)
        p1[c].forward(1)
    kvz_wait(2)
    kvy_start(2)
    kvy_forward(3)
    kvy_forward(1)
    for c in range(3):
        p1[c].finish()
        p2[c].start()
        p3[c][0].start()
    kvy_forward(2)
    for rel in (0, 3, 1, 2):
        kvy_finish(rel)

    scale = float(HEAD_DIM ** -0.5 * np.log2(np.e))
    lam = jnp.concatenate(
        [jnp.full((1, 128), lam_ref[me["z"] * GROUP + h], f32) for h in range(GROUP)], 1
    )
    lane = lax.broadcasted_iota(jnp.int32, (128, 128), 1)
    half_rows = GROUP * ROWS

    def attend(i):
        zq = lax.rem(me["z"] + 1 + i, 4)
        if i < 3:
            o = 3 - i
            arrived(qin.at[zq], qz_s.at[o - 1], qz_r.at[o - 1])
        for m in range(2):
            keep = (lane < 64) if m == 0 else (lane >= 64)
            for h in range(GROUP):
                part = qin[zq, :, h * 128:(h + 1) * 128]
                q2[(m * GROUP + h) * 128:(m * GROUP + h + 1) * 128, :] = jnp.where(
                    keep, part, jnp.zeros_like(part)
                )
        block = zq * 4 + me["y"]
        last = block // 2

        def scores(t):
            keys = jnp.concatenate([kv[2 * t, 0], kv[2 * t + 1, 0]], 0)
            return lax.dot_general(keys, q2[...], (((1,), (1,)), ((), ())), preferred_element_type=f32)

        def fold(x, op):
            r = x.reshape(KT // 8, 8, x.shape[1])
            return op(r, 0)

        def pass1(t, top):
            s = scores(t)
            sbuf[t] = s
            return jnp.maximum(top, fold(s, jnp.max))

        top = lax.fori_loop(0, last, pass1, jnp.full((8, 2 * half_rows), -1e30, f32))
        s = scores(last)
        key_at = lax.broadcasted_iota(jnp.int32, (KT, 2 * half_rows), 0) + last * KT
        query_at = lax.rem(lax.broadcasted_iota(jnp.int32, (KT, 2 * half_rows), 1), 128) + block * 128
        s = jnp.where(key_at <= query_at, s, -1e30)
        sbuf[last] = s
        top = jnp.maximum(top, fold(s, jnp.max))
        top = jnp.max(top, 0, keepdims=True)

        def pass2(t, total):
            p = jnp.exp2((sbuf[t] - top) * scale)
            sbuf[t] = p
            return total + fold(p, jnp.sum)

        total = lax.fori_loop(0, last + 1, pass2, jnp.zeros((8, 2 * half_rows), f32))
        total = jnp.sum(total, 0, keepdims=True)
        a0 = 1.0 / total[:, :half_rows]
        a1 = lam / total[:, half_rows:]
        acc[...] = jnp.zeros_like(acc)

        def pass3(t, carry):
            w = (sbuf[t, :, :half_rows] * a0 - sbuf[t, :, half_rows:] * a1).astype(bf16)
            vals = jnp.concatenate([kv[2 * t, 1], kv[2 * t + 1, 1]], 1)
            acc[...] += jnp.dot(vals, w, preferred_element_type=f32)
            return carry

        lax.fori_loop(0, last + 1, pass3, 0)
        hv = acc[...]
        inv = lax.rsqrt(jnp.mean(hv * hv, 0, keepdims=True) + NORM_EPS)
        hv = hv * inv
        for h in range(GROUP):
            piece = hv[:, h * 128:(h + 1) * 128].T
            hst[zq, :, h * 128:(h + 1) * 128] = (piece * gain_ref[...] * OUTPUT_SCALE).astype(bf16)
        return zq

    def ship(i, zq):
        if i < 3:
            o = i + 1
            send(hst.at[zq], acts.at[0, me["z"]], oz_s.at[o - 1], oz_r.at[o - 1], at(shift("z", o)))
        else:
            acts[0, me["z"]] = hst[me["z"]]
            send(hst.at[me["z"]], acts.at[1, me["z"]], af_s.at[3], af_r.at[3], partner)

    zq = attend(0)
    ship(0, zq)
    for c in range(3):
        p2[c].forward(0)
        p3[c][3].start()
    zq = attend(1)
    ship(1, zq)
    for c in range(3):
        p2[c].forward(1)
        p3[c][1].start()
    zq = attend(2)
    ship(2, zq)
    for c in range(3):
        p3[c][0].forward(0)
        p3[c][0].forward(1)
        p2[c].finish()
        p3[c][2].start()
    zq = attend(3)
    ship(3, zq)
    for o in (1, 2, 3):
        g = lax.rem(me["z"] + 4 - o, 4)
        arrived(acts.at[0, g], oz_s.at[o - 1], oz_r.at[o - 1])
        send(acts.at[0, g], acts.at[1, g], af_s.at[o - 1], af_r.at[o - 1], partner)
    for r in (3, 1, 2):
        for c in range(3):
            p3[c][r].forward(0)
            p3[c][r].forward(1)
    for o in (1, 2, 3):
        g = lax.rem(me["z"] + 4 - o, 4)
        arrived(acts.at[1, g], af_s.at[o - 1], af_r.at[o - 1])
    arrived(acts.at[1, me["z"]], af_s.at[3], af_r.at[3])
    for r in (0, 3, 1, 2):
        for c in range(3):
            p3[c][r].finish()

    def project(n):
        total = None
        weights = wbuf[n].reshape(512, 2048)
        for g in range(KV_HEADS):
            left = acts[:, g].reshape(2 * ROWS, 512)
            part = lax.dot_general(
                left, weights[:, g * 512:(g + 1) * 512], (((1,), (1,)), ((), ())), preferred_element_type=f32
            )
            total = part if total is None else total + part
        oown[n] = total[:ROWS].astype(bf16)
        opart[n] = total[ROWS:].astype(bf16)

    for n in range(4):
        project(n)
        send(opart.at[n], oin.at[n], oo_s.at[n], oo_r.at[n], partner)

    erow = lax.broadcasted_iota(jnp.int32, (256, 256), 0)
    ecol = lax.broadcasted_iota(jnp.int32, (256, 256), 1)
    mine = jnp.where(erow < 128, core, 1 - core)
    er = lax.rem(erow, 128)
    spread = jnp.where(ecol == (er // 32) * 64 + mine * 32 + lax.rem(er, 32), 1.0, 0.0).astype(bf16)
    for n in range(4):
        arrived(oin.at[n], oo_s.at[n], oo_r.at[n])
        for b in range(4):
            both = jnp.concatenate([oown[n, :, b * 128:(b + 1) * 128], oin[n, :, b * 128:(b + 1) * 128]], 1)
            a = (n * 4 + b) * 256
            out_ref[:, a:a + 256] = jnp.dot(both, spread, preferred_element_type=f32).astype(bf16)
    for copy in pending:
        copy.wait_send()


def shards(queries, keys, values, lambdas, value_gain, out_weight):
    inner, outer = rotation_tables()
    vmem = pl.BlockSpec(memory_space=pltpu.VMEM)
    smem = pl.BlockSpec(memory_space=pltpu.SMEM)
    hbm = pl.BlockSpec(memory_space=pl.ANY)
    bf16, f32 = jnp.bfloat16, jnp.float32
    dma = lambda n: pltpu.SemaphoreType.DMA((n,))
    out = pl.pallas_call(
        kernel,
        out_shape=jax.ShapeDtypeStruct((ROWS, D), bf16),
        in_specs=[smem, hbm, hbm, hbm, vmem, vmem, vmem, hbm],
        out_specs=vmem,
        scratch_shapes=[
            pltpu.VMEM((ROWS, 2048), bf16),
            pltpu.VMEM((ROWS, 512), bf16),
            pltpu.VMEM((ROWS, 512), bf16),
            pltpu.VMEM((4, 2, 128, 128), bf16),
            pltpu.VMEM((16, 2, 128, 128), bf16),
            pltpu.VMEM((4, 128, 512), bf16),
            pltpu.VMEM((4, 128, 512), bf16),
            pltpu.VMEM((1024, 128), bf16),
            pltpu.VMEM((8, KT, 1024), f32),
            pltpu.VMEM((128, 512), f32),
            pltpu.VMEM((4, 4, 4, 32, 2048), bf16),
            pltpu.VMEM((4, 128, 512), bf16),
            pltpu.VMEM((2, 4, 128, 512), bf16),
            pltpu.VMEM((4, 128, 512), bf16),
            pltpu.VMEM((4, 128, 512), bf16),
            pltpu.VMEM((4, 128, 512), bf16),
            dma(4), dma(3), dma(3), dma(16), dma(16), dma(3), dma(3), dma(72), dma(72),
            dma(3), dma(3), dma(4), dma(4), dma(4), dma(4),
        ],
        compiler_params=pltpu.CompilerParams(
            collective_id=0, has_side_effects=True, vmem_limit_bytes=48 * 1024 * 1024
        ),
        name="layer",
    )(
        lambdas, queries[0], keys[0], values[0], value_gain.reshape(1, 128),
        jnp.asarray(inner), jnp.asarray(outer), out_weight.T,
    )
    return out[None]


def solution(mesh):
    return jax.shard_map(
        shards,
        mesh=mesh,
        in_specs=(
            P("dp", "sp", None),
            P("dp", "sp", None),
            P("dp", "sp", None),
            P(),
            P(),
            P(None, ("sp", "dp")),
        ),
        out_specs=P("dp", "sp", None),
        check_vma=False,
    )
```

time: 125 us -> 71.7 us (0.57)
  the two profiles are of different devices: /device:TPU:2 before, /device:TPU:1 now
where the time goes in v1:
time: 71.7 us; the launch traced here: 71.4 us
  Pallas kernels  64.4 us (90%)
  local copies, waits for them, and re-layouts  7.01 us (10%)
    pallas_call x1, Pallas kernels, shards(): pl.pallas_call(kernel, out_shape=jax.ShapeDtypeStruct((ROWS, D), bf16), i...  64.4 us
    unnamed x17, local copies, waits for them, and re-layouts  7.01 us

profile of v1, /device:TPU:1, one launch (start us, length us, event | category | flops | bytes accessed | tf_op | source)
XLA Modules:
  0.0 71.4 jit_solution(9783342681654821350)
XLA Ops:
  0.0 0.0 copy-start.6
  0.0 0.0 copy-start.7
  0.0 0.7 copy-done.6
  0.7 0.0 copy-done.7
  0.7 0.0 copy-start
  0.7 1.0 %copy-done = bf16[1,128,2048]{2,1,0:T(8,128)(2,1)S(1)} copy-done((bf16[1,128,2048]{2,1,0:T(8,128)(2,1)S(1)}, bf16[1,128,2048]{2,1,0:T(8,128)(2,1)}, u32[]{:S(2)}) %copy-start) | copy-done | bytes 524312
  1.7 0.0 copy-start.1
  1.7 0.9 %copy-done.1 = bf16[1,128,512]{2,1,0:T(8,128)(2,1)S(1)} copy-done((bf16[1,128,512]{2,1,0:T(8,128)(2,1)S(1)}, bf16[1,128,512]{2,1,0:T(8,128)(2,1)}, u32[]{:S(2)}) %copy-start.1) | copy-done | bytes 131096
  2.6 0.0 copy-start.2
  2.6 0.9 %copy-done.2 = bf16[1,128,512]{2,1,0:T(8,128)(2,1)S(1)} copy-done((bf16[1,128,512]{2,1,0:T(8,128)(2,1)S(1)}, bf16[1,128,512]{2,1,0:T(8,128)(2,1)}, u32[]{:S(2)}) %copy-start.2) | copy-done | bytes 131096
  3.5 0.0 copy-start.3
  3.5 0.9 %copy-done.3 = bf16[2048,32]{0,1:T(8,128)(2,1)S(1)} copy-done((bf16[2048,32]{0,1:T(8,128)(2,1)S(1)}, bf16[2048,32]{0,1:T(8,128)(2,1)}, u32[]{:S(2)}) %copy-start.3) | copy-done | bytes 131096
  4.4 0.0 copy-start.4
  4.4 0.9 %copy-done.4 = f32[2,128,128]{2,1,0:T(8,128)S(1)} copy-done((f32[2,128,128]{2,1,0:T(8,128)S(1)}, f32[2,128,128]{2,1,0:T(8,128)}, u32[]{:S(2)}) %copy-start.4) | copy-done | bytes 131096
  5.3 0.0 copy-start.5
  5.3 0.7 %copy-done.5 = f32[16,2,128]{2,1,0:T(2,128)S(1)} copy-done((f32[16,2,128]{2,1,0:T(2,128)S(1)}, f32[16,2,128]{2,1,0:T(2,128)}, u32[]{:S(2)}) %copy-start.5) | copy-done | bytes 16408
  6.1 64.4 %layer.1 = bf16[128,4096]{1,0:T(8,128)(2,1)S(1)} custom-call(f32[16]{0:T(128)S(1)} %copy-done.6, bf16[128,2048]{1,0:T(8,128)(2,1)S(1)} %bitcast.7, bf16[128,512]{1,0:T(8,128)(2,1)S(1)} %bitcast.8, bf16[128,512]{1,0:T(8,128)(2,1)S(1)} %bitcast.9, f32[1,128]{1,0:T(1,128)S(1)} %bitcast.11, f32[2,128,128]{2,1,0:T(8,128)S(1)} %copy-done.4, ...), custom_call_target="tpu_custom_call" | custom-call | tf_op jit(solution)/shard_map/layer/pallas_call | solution.py:382
  70.4 1.0 %copy.10 = bf16[1,128,4096]{2,1,0:T(8,128)(2,1)} copy(bf16[1,128,4096]{2,1,0:T(8,128)(2,1)S(1)} %bitcast.6) | data formatting | bytes 2097152
Async XLA Ops:
  0.0 0.7 copy-start.6
  0.0 0.7 copy-start.7
  0.7 1.0 %copy-start = (bf16[1,128,2048]{2,1,0:T(8,128)(2,1)S(1)}, bf16[1,128,2048]{2,1,0:T(8,128)(2,1)}, u32[]{:S(2)}) copy-start(bf16[1,128,2048]{2,1,0:T(8,128)(2,1)} %param.8) | copy-start | bytes 1572868
  1.7 0.9 %copy-start.1 = (bf16[1,128,512]{2,1,0:T(8,128)(2,1)S(1)}, bf16[1,128,512]{2,1,0:T(8,128)(2,1)}, u32[]{:S(2)}) copy-start(bf16[1,128,512]{2,1,0:T(8,128)(2,1)} %param.9) | copy-start | bytes 393220
  2.6 0.9 %copy-start.2 = (bf16[1,128,512]{2,1,0:T(8,128)(2,1)S(1)}, bf16[1,128,512]{2,1,0:T(8,128)(2,1)}, u32[]{:S(2)}) copy-start(bf16[1,128,512]{2,1,0:T(8,128)(2,1)} %param.10) | copy-start | bytes 393220
  3.5 0.9 %copy-start.3 = (bf16[2048,32]{0,1:T(8,128)(2,1)S(1)}, bf16[2048,32]{0,1:T(8,128)(2,1)}, u32[]{:S(2)}) copy-start(bf16[2048,32]{0,1:T(8,128)(2,1)} %param.13) | copy-start | bytes 393220
  4.4 0.9 %copy-start.4 = (f32[2,128,128]{2,1,0:T(8,128)S(1)}, f32[2,128,128]{2,1,0:T(8,128)}, u32[]{:S(2)}) copy-start(f32[2,128,128]{2,1,0:T(8,128)} %constant.4.clone.inner_ref) | copy-start | bytes 393220
  5.3 0.7 %copy-start.5 = (f32[16,2,128]{2,1,0:T(2,128)S(1)}, f32[16,2,128]{2,1,0:T(2,128)}, u32[]{:S(2)}) copy-start(f32[16,2,128]{2,1,0:T(2,128)} %constant.5.clone.outer_ref) | copy-start | bytes 49156

commit v2 on v1

v2 whole, which is shorter than its diff:
```python
import functools

import jax
import jax.numpy as jnp
import numpy as np
from jax import lax
from jax.experimental import pallas as pl
from jax.experimental.pallas import tpu as pltpu
from jax.sharding import PartitionSpec as P

HEADS = 16
KV_HEADS = 4
HEAD_DIM = 64
VALUE_DIM = 128
D = 4096
SEQLEN = 2048
ROWS = 128
GROUP = HEADS // KV_HEADS
KT = 512
ROPE_BASE = 500000.0
OUTPUT_SCALE = 0.8
NORM_EPS = 1e-05
MESH = pl.DeviceIdType.MESH

COLOURS = ((0, 1024), (1024, 512), (1536, 512))


def rotation_tables():
    f32 = np.float32
    freqs = (f32(ROPE_BASE) ** (-np.arange(0, HEAD_DIM, 2, dtype=f32) / f32(HEAD_DIM))).astype(f32)
    lanes = np.tile(freqs.astype(np.float64), 4)
    inner = np.arange(ROWS)[:, None] * lanes[None]
    outer = (np.arange(SEQLEN // ROWS) * ROWS)[:, None] * lanes[None]
    inner = np.stack([np.cos(inner), np.sin(inner)]).astype(f32)
    outer = np.stack([np.cos(outer), np.sin(outer)], 1).astype(f32)
    return inner, outer


def kernel(
    lam_hbm, q_hbm, k_hbm, v_hbm, gain_hbm, inner_hbm, outer_hbm, w_hbm,
    out_ref,
    lam_ref, gain_ref, inner_ref, outer_ref, q_in, k_in, v_in,
    kvst, kv, qst, qin, q2, sbuf, acc, wbuf, hst, acts, pacc, oown, opart, oin,
    in_sem, sent, kvz_r, kvy_r, q_r, ring_r, fin_r, oz_r, af_r, oo_r,
):
    f32, bf16 = jnp.float32, jnp.bfloat16
    sp, dp = lax.axis_index("sp"), lax.axis_index("dp")
    me = {"z": sp // 4, "y": lax.rem(sp, 4), "x": dp // 2}
    core = lax.rem(dp, 2)

    def at(pos):
        return (pos["z"] * 4 + pos["y"], pos["x"] * 2 + core)

    def shift(dim, off):
        return {**me, dim: lax.rem(me[dim] + off + 4, 4)}

    partner = (sp, me["x"] * 2 + 1 - core)
    total_sent = [0, 0]

    def size(ref):
        return int(np.prod(ref.shape)) * ref.dtype.itemsize

    def amount(nbytes):
        rows = nbytes // 4096
        n = 1 if rows <= KT else (2 if rows % 16 == 0 and rows <= 2 * KT else 4)
        assert rows * 4096 == nbytes and rows % n == 0
        return sbuf.at[pl.ds(0, n), pl.ds(0, rows // n), :]

    def send(src, dst, r_sem, dev, kind=0):
        total_sent[kind] += size(src)
        pltpu.make_async_remote_copy(
            src_ref=src, dst_ref=dst, send_sem=sent.at[kind], recv_sem=r_sem, device_id=dev, device_id_type=MESH
        ).start()

    def arrived(nbytes, r_sem, name="wait"):
        view = amount(nbytes)
        with jax.named_scope(name):
            pltpu.make_async_remote_copy(
                src_ref=view, dst_ref=view, send_sem=sent.at[0], recv_sem=r_sem, device_id=partner, device_id_type=MESH
            ).wait_recv()

    barrier = pltpu.get_barrier_semaphore()
    peers = [at(shift("z", o)) for o in (1, 2, 3)] + [at(shift("y", o)) for o in (1, 3)]
    peers += [at(shift("x", o)) for o in (1, 3)] + [partner]
    for dev in peers:
        pl.semaphore_signal(barrier, inc=1, device_id=dev, device_id_type=MESH)

    copies = [
        pltpu.make_async_copy(src, dst, in_sem.at[n])
        for n, (src, dst) in enumerate((
            (k_hbm, k_in),
            (inner_hbm, inner_ref),
            (outer_hbm.at[sp], outer_ref),
            (v_hbm, v_in),
            (w_hbm, wbuf.at[me["z"], me["y"], me["x"]]),
            (q_hbm, q_in),
            (gain_hbm, gain_ref),
            (lam_hbm, lam_ref),
        ))
    ]
    for c in copies:
        c.start()
    c_k, c_in, c_out, c_v, c_w, c_q, c_gain, c_lam = copies
    c_in.wait()
    c_out.wait()

    ci, si = inner_ref[0], inner_ref[1]
    co, so = outer_ref[0:1, :], outer_ref[1:2, :]
    cosine = co * ci - so * si
    sine = so * ci + co * si
    row = lax.broadcasted_iota(jnp.int32, (128, 128), 0)
    col = lax.broadcasted_iota(jnp.int32, (128, 128), 1)
    low = lax.rem(col, 64) < 32
    swap = jnp.where(
        low & (row == col + 32), -1.0, jnp.where(jnp.logical_not(low) & (row == col - 32), 1.0, 0.0)
    ).astype(bf16)

    def rotate(part):
        turned = jnp.dot(part, swap, preferred_element_type=f32)
        return (part.astype(f32) * cosine + turned * sine).astype(bf16)

    with jax.named_scope("rotk"):
        c_k.wait()
        c_v.wait()
        for g in range(KV_HEADS):
            cols = slice(g * 128, (g + 1) * 128)
            kvst[g, 0] = rotate(k_in[:, cols])
            kvst[g, 1] = v_in[:, cols].astype(f32).T.astype(bf16)
    kv[sp, 0] = kvst[me["z"], 0]
    kv[sp, 1] = kvst[me["z"], 1]
    with jax.named_scope("barrier"):
        pl.semaphore_wait(barrier, len(peers))

    steps = (0, 3, 1, 2)
    block_bytes = size(kv.at[0])

    def kv_block(rel, off):
        return lax.rem(me["z"] + rel, 4) * 4 + lax.rem(me["y"] + off + 4, 4)

    def kvz_start(o):
        pos = shift("z", o)
        send(kvst.at[pos["z"]], kv.at[sp], kvz_r.at[o - 1], at(pos))

    def kvz_wait(rel):
        arrived(block_bytes, kvz_r.at[3 - rel], f"kvz_{rel}")

    def kvy_start(rel):
        view = kvst.at[me["z"]] if rel == 0 else kv.at[kv_block(rel, 0)]
        for off in (1, -1):
            send(view, kv.at[kv_block(rel, 0)], kvy_r.at[rel], at(shift("y", off)))

    def kvy_forward(rel):
        arrived(2 * block_bytes, kvy_r.at[rel], f"kvy_{rel}")
        for n, off in enumerate((-1, 1)):
            half = kv.at[kv_block(rel, off), n]
            send(half, half, kvy_r.at[4], at(shift("y", -off)))

    made = []

    class Ring:
        def __init__(self, colour, dim, fin, **fixed):
            self.dim, self.fixed = dim, fixed
            self.k0, self.kn = COLOURS[colour]
            self.full, self.fin = ring_r.at[len(made)], fin_r.at[fin]
            self.bytes = size(self.view(0))
            self.name = f"{len(made)}{dim}"
            made.append(self)

        def view(self, off, half=None):
            sel, rows = {}, slice(None)
            for d in "zyx":
                rel = off if d == self.dim else self.fixed[d]
                sel[d] = slice(None) if rel is None else lax.rem(me[d] + rel + 4, 4)
            if half is not None:
                free = [d for d in "zyx" if d != self.dim and self.fixed[d] is None]
                if free:
                    sel[free[0]] = pl.ds(2 * half, 2)
                else:
                    rows = pl.ds(16 * half, 16)
            return wbuf.at[sel["z"], sel["y"], sel["x"], rows, pl.ds(self.k0, self.kn)]

        def start(self):
            view = self.view(0)
            for off in (1, -1):
                send(view, view, self.full, at(shift(self.dim, off)), 1)

        def forward(self):
            arrived(2 * self.bytes, self.full, "fwd" + self.name)
            for n, off in enumerate((-1, 1)):
                half = self.view(off, n)
                send(half, half, self.fin, at(shift(self.dim, -off)), 1)

        def finish(self):
            arrived(self.bytes, self.fin, "fin" + self.name)

    x1 = Ring(0, "z", 0, y=0, x=0)
    x2 = {a: Ring(0, "y", 1 + a, z=a, x=0) for a in steps}
    x3 = {(a, b): Ring(0, "x", 5 + b, z=a, y=b) for b in steps for a in steps}
    y1 = Ring(1, "x", 9, z=0, y=0)
    y2 = Ring(1, "z", 10, x=None, y=0)
    y3 = {a: Ring(1, "y", 11 + a, x=None, z=a) for a in steps}
    z1 = Ring(2, "x", 15, z=0, y=0)
    z2 = Ring(2, "y", 16, x=None, z=0)
    z3 = {b: Ring(2, "z", 17 + b, x=None, y=b) for b in steps}

    def x3_finish(b):
        arrived(4 * x3[0, b].bytes, x3[0, b].fin, f"finx{b}")

    c_w.wait()
    for ring in (x1, x2[0], x3[0, 0], y1, z1):
        ring.start()
    for o in (1, 3, 2):
        kvz_start(o)
    kvy_start(0)

    with jax.named_scope("rotq"):
        c_q.wait()
        for g in range(KV_HEADS):
            for h in range(GROUP):
                a = (g * GROUP + h) * 128
                qst[g, :, h * 128:(h + 1) * 128] = rotate(q_in[:, a:a + 128])
    qin[me["z"]] = qst[me["z"]]
    x1.forward()
    for ring in (x3[3, 0], x3[1, 0]):
        ring.start()
    kvz_wait(3)
    kvy_start(3)
    kvz_wait(1)
    kvy_start(1)
    for o in (1, 3, 2):
        pos = shift("z", o)
        send(qst.at[pos["z"]], qin.at[me["z"]], q_r.at[o - 1], at(pos))
    x2[0].forward()
    for ring in (x3[0, 3], x3[0, 1]):
        ring.start()
    y1.forward()
    z1.forward()
    kvy_forward(0)
    for ring in (x2[3], x2[1]):
        ring.start()
    x3[0, 0].forward()
    x1.finish()
    x3[2, 0].start()
    kvz_wait(2)
    kvy_start(2)
    x2[2].start()
    y1.finish()
    z1.finish()
    y2.start()
    z3[0].start()
    kvy_forward(3)
    kvy_forward(1)
    x2[0].finish()
    x3[0, 2].start()
    x3[3, 0].forward()
    x3[1, 0].forward()
    for a in (3, 1):
        x2[a].forward()
        x3[a, 3].start()
        x3[a, 1].start()
    kvy_forward(2)
    pacc[...] = jnp.zeros_like(pacc)
    z2.start()
    y3[0].start()
    x3[0, 3].forward()
    x3[0, 1].forward()
    arrived(4 * block_bytes, kvy_r.at[4], "kvyf")

    scale = float(HEAD_DIM ** -0.5 * np.log2(np.e))
    c_lam.wait()
    lam = jnp.concatenate(
        [jnp.full((1, 128), lam_ref[me["z"] * GROUP + h], f32) for h in range(GROUP)], 1
    )
    lane = lax.broadcasted_iota(jnp.int32, (128, 128), 1)
    half_rows = GROUP * ROWS

    def attend(i, after):
        zq = lax.rem(me["z"] + 1 + i, 4)
        if i < 3:
            o = 3 - i
            arrived(size(qin.at[0]), q_r.at[o - 1], f"q_{i}")
        for m in range(2):
            keep = (lane < 64) if m == 0 else (lane >= 64)
            for h in range(GROUP):
                part = qin[zq, :, h * 128:(h + 1) * 128]
                q2[(m * GROUP + h) * 128:(m * GROUP + h + 1) * 128, :] = jnp.where(
                    keep, part, jnp.zeros_like(part)
                )
        block = zq * 4 + me["y"]
        last = zq

        def scores(t):
            keys = jnp.concatenate([kv[4 * t + b, 0] for b in range(4)], 0)
            return lax.dot_general(keys, q2[...], (((1,), (1,)), ((), ())), preferred_element_type=f32)

        def fold(x, op):
            r = x.reshape(KT // 8, 8, x.shape[1])
            return op(r, 0)

        def pass1(t, top):
            s = scores(t)
            sbuf[t] = s
            return jnp.maximum(top, fold(s, jnp.max))

        scope = jax.named_scope(f"pass1_{i}")
        scope.__enter__()
        top = lax.fori_loop(0, last, pass1, jnp.full((8, 2 * half_rows), -1e30, f32))
        s = scores(last)
        key_at = lax.broadcasted_iota(jnp.int32, (KT, 2 * half_rows), 0) + last * KT
        query_at = lax.rem(lax.broadcasted_iota(jnp.int32, (KT, 2 * half_rows), 1), 128) + block * 128
        s = jnp.where(key_at <= query_at, s, -1e30)
        sbuf[last] = s
        top = jnp.maximum(top, fold(s, jnp.max))
        top = jnp.max(top, 0, keepdims=True)
        scope.__exit__(None, None, None)
        after[0]()

        def pass2(t, total):
            p = jnp.exp2((sbuf[t] - top) * scale)
            sbuf[t] = p
            return total + fold(p, jnp.sum)

        with jax.named_scope(f"pass2_{i}"):
            total = lax.fori_loop(0, last + 1, pass2, jnp.zeros((8, 2 * half_rows), f32))
        after[1]()
        total = jnp.sum(total, 0, keepdims=True)
        a0 = 1.0 / total[:, :half_rows]
        a1 = lam / total[:, half_rows:]
        acc[...] = jnp.zeros_like(acc)

        def pass3(t, carry):
            w = (sbuf[t, :, :half_rows] * a0 - sbuf[t, :, half_rows:] * a1).astype(bf16)
            vals = jnp.concatenate([kv[4 * t + b, 1] for b in range(4)], 1)
            acc[...] += jnp.dot(vals, w, preferred_element_type=f32)
            return carry

        with jax.named_scope(f"pass3_{i}"):
            lax.fori_loop(0, last + 1, pass3, 0)
        after[2]()
        hv = acc[...]
        inv = lax.rsqrt(jnp.mean(hv * hv, 0, keepdims=True) + NORM_EPS)
        hv = hv * inv
        for h in range(GROUP):
            piece = hv[:, h * 128:(h + 1) * 128].T
            hst[zq, :, h * 128:(h + 1) * 128] = (piece * gain_ref[...] * OUTPUT_SCALE).astype(bf16)
        return zq

    def ship(i, zq):
        if i < 3:
            o = i + 1
            send(hst.at[zq], acts.at[0, me["z"]], oz_r.at[o - 1], at(shift("z", o)))
        else:
            acts[0, me["z"]] = hst[me["z"]]
            send(hst.at[me["z"]], acts.at[1, me["z"]], af_r.at[0], partner)

    def acts_in(o):
        g = lax.rem(me["z"] + 4 - o, 4)
        arrived(size(acts.at[0, 0]), oz_r.at[o - 1], f"o_{o}")
        send(acts.at[0, g], acts.at[1, g], af_r.at[0], partner)

    def multiply(heads, weights):
        total = None
        for n, g in enumerate(heads):
            part = lax.dot_general(
                acts[:, g].reshape(2 * ROWS, 512), weights[:, n * 512:(n + 1) * 512],
                (((1,), (1,)), ((), ())), preferred_element_type=f32,
            )
            total = part if total is None else total + part
        return total

    def project_xz(b):
        with jax.named_scope(f"proj_xz{b}"):
            yb = lax.rem(me["y"] + b, 4)
            cat = lambda lo, hi: jnp.concatenate(
                [wbuf[z, yb, :, :, lo:hi].reshape(128, hi - lo) for z in range(4)], 0
            )
            part = multiply((0, 1), cat(0, 1024)) + multiply((3,), cat(1536, 2048))
            for z in range(4):
                pacc[z, yb] += part[:, z * 128:(z + 1) * 128]

    def project_y(a):
        with jax.named_scope(f"proj_y{a}"):
            za = lax.rem(me["z"] + a, 4)
            part = multiply((2,), wbuf[za, :, :, :, 1024:1536].reshape(512, 512))
            for y in range(4):
                pacc[za, y] += part[:, y * 128:(y + 1) * 128]

    early = [(a, b) for a in (0, 3, 1) for b in (0, 3, 1)]
    late = [(2, b) for b in (0, 3, 1)] + [(a, 2) for a in steps]

    def tile_of(a, b):
        return lax.rem(me["z"] + a, 4), lax.rem(me["y"] + b, 4)

    def swap_tiles(tiles, n):
        for a, b in tiles:
            z, y = tile_of(a, b)
            opart[z, y] = pacc[z, y, ROWS:].astype(bf16)
        for a, b in tiles:
            z, y = tile_of(a, b)
            send(opart.at[z, y], oin.at[z, y], oo_r.at[n], partner)
            oown[z, y] = pacc[z, y, :ROWS].astype(bf16)

    erow = lax.broadcasted_iota(jnp.int32, (256, 256), 0)
    ecol = lax.broadcasted_iota(jnp.int32, (256, 256), 1)
    mine = jnp.where(erow < 128, core, 1 - core)
    er = lax.rem(erow, 128)
    spread = jnp.where(ecol == (er // 32) * 64 + mine * 32 + lax.rem(er, 32), 1.0, 0.0).astype(bf16)

    def merge(tiles, n):
        arrived(len(tiles) * size(oin.at[0, 0]), oo_r.at[n], f"swap_{n}")
        with jax.named_scope(f"merge_{n}"):
            for a, b in tiles:
                z, y = tile_of(a, b)
                both = jnp.concatenate([oown[z, y], oin[z, y]], 1)
                cols = pl.ds(pl.multiple_of((z * 4 + y) * 256, 256), 256)
                out_ref[:, cols] = jnp.dot(both, spread, preferred_element_type=f32).astype(bf16)

    def nothing():
        pass

    def h00():
        x2[2].forward()
        x3[2, 3].start()
        x3[2, 1].start()

    def h01():
        for a in (3, 1):
            x2[a].finish()
            x3[a, 2].start()
        x3[2, 0].forward()

    def h10():
        y2.forward()
        y3[3].start()
        y3[1].start()
        x3[0, 2].forward()

    def h11():
        x2[2].finish()
        x3[2, 2].start()
        z2.forward()
        z3[3].start()
        z3[1].start()

    def h12():
        x3[3, 3].forward()

    def h20():
        x3[3, 1].forward()
        z3[0].forward()

    def h21():
        y2.finish()
        y3[2].start()

    def h22():
        z2.finish()
        z3[2].start()
        y3[0].forward()
        x3[1, 3].forward()

    def h30():
        x3[1, 1].forward()
        x3[2, 3].forward()

    c_gain.wait()
    hooks = ((h00, h01, nothing), (h10, h11, h12), (h20, h21, h22), (h30, nothing, nothing))
    for i in range(4):
        ship(i, attend(i, hooks[i]))
    acts_in(1)
    x3[2, 1].forward()
    acts_in(2)
    acts_in(3)
    z3[3].forward()
    y3[3].forward()
    x3_finish(0)
    z3[0].finish()
    x3[3, 2].forward()
    arrived(4 * size(acts.at[0, 0]), af_r.at[0], "acts")
    project_xz(0)
    z3[1].forward()
    y3[1].forward()
    x3[1, 2].forward()
    y3[0].finish()
    project_y(0)
    x3[2, 2].forward()
    x3_finish(3)
    z3[3].finish()
    project_xz(3)
    z3[2].forward()
    y3[2].forward()
    y3[3].finish()
    project_y(3)
    x3_finish(1)
    z3[1].finish()
    project_xz(1)
    y3[1].finish()
    project_y(1)
    swap_tiles(early, 0)
    x3_finish(2)
    z3[2].finish()
    project_xz(2)
    y3[2].finish()
    project_y(2)
    swap_tiles(late, 1)
    merge(early, 0)
    merge(late, 1)
    with jax.named_scope("drain"):
        for kind in (0, 1):
            view = amount(total_sent[kind])
            pltpu.make_async_remote_copy(
                src_ref=view, dst_ref=view, send_sem=sent.at[kind], recv_sem=oo_r.at[0],
                device_id=partner, device_id_type=MESH,
            ).wait_send()


def shards(queries, keys, values, lambdas, value_gain, out_weight):
    inner, outer = rotation_tables()
    vmem = pl.BlockSpec(memory_space=pltpu.VMEM)
    hbm = pl.BlockSpec(memory_space=pltpu.HBM)
    bf16, f32 = jnp.bfloat16, jnp.float32
    dma = lambda n: pltpu.SemaphoreType.DMA((n,))
    out = pl.pallas_call(
        kernel,
        out_shape=jax.ShapeDtypeStruct((ROWS, D), bf16),
        in_specs=[hbm] * 8,
        out_specs=vmem,
        scratch_shapes=[
            pltpu.SMEM((HEADS,), f32),
            pltpu.VMEM((1, 128), f32),
            pltpu.VMEM((2, ROWS, 128), f32),
            pltpu.VMEM((2, 128), f32),
            pltpu.VMEM((ROWS, 2048), bf16),
            pltpu.VMEM((ROWS, 512), bf16),
            pltpu.VMEM((ROWS, 512), bf16),
            pltpu.VMEM((4, 2, 128, 128), bf16),
            pltpu.VMEM((16, 2, 128, 128), bf16),
            pltpu.VMEM((4, 128, 512), bf16),
            pltpu.VMEM((4, 128, 512), bf16),
            pltpu.VMEM((1024, 128), bf16),
            pltpu.VMEM((SEQLEN // KT, KT, 1024), f32),
            pltpu.VMEM((128, 512), f32),
            pltpu.VMEM((4, 4, 4, 32, 2048), bf16),
            pltpu.VMEM((4, 128, 512), bf16),
            pltpu.VMEM((2, 4, 128, 512), bf16),
            pltpu.VMEM((4, 4, 256, 128), f32),
            pltpu.VMEM((4, 4, 128, 128), bf16),
            pltpu.VMEM((4, 4, 128, 128), bf16),
            pltpu.VMEM((4, 4, 128, 128), bf16),
            dma(8), dma(2), dma(3), dma(5), dma(3), dma(33), dma(21), dma(3), dma(1), dma(2),
        ],
        compiler_params=pltpu.CompilerParams(
            collective_id=0, has_side_effects=True, vmem_limit_bytes=50_000_000
        ),
        name="layer",
    )(*(
        pltpu.with_memory_space_constraint(a, pltpu.HBM)
        for a in (
            lambdas, queries[0], keys[0], values[0], value_gain.reshape(1, 128),
            jnp.asarray(inner), jnp.asarray(outer), out_weight.T,
        )
    ))
    return out[None]


def solution(mesh):
    return jax.shard_map(
        shards,
        mesh=mesh,
        in_specs=(
            P("dp", "sp", None),
            P("dp", "sp", None),
            P("dp", "sp", None),
            P(),
            P(),
            P(None, ("sp", "dp")),
        ),
        out_specs=P("dp", "sp", None),
        check_vma=False,
    )
```

time: 71.7 us -> 62.8 us (0.88)
  local copies, waits for them, and re-layouts: 7.01 us -> 0.97 us
  Pallas kernels: 64.4 us -> 61.7 us
    unnamed x17 -> x1, local copies, waits for them, and re-layouts: 7.01 us -> 0.97 us
    pallas_call x1, Pallas kernels: 64.4 us -> 61.7 us  [shards(): pl.pallas_call(kernel, out_shape=jax.ShapeDtypeStruct((ROWS, D), bf16), i...]
where the time goes in v2:
time: 62.8 us; the launch traced here: 62.7 us
  Pallas kernels  61.7 us (98%)
  local copies, waits for them, and re-layouts  0.97 us (2%)
    pallas_call x1, Pallas kernels, shards(): pl.pallas_call(kernel, out_shape=jax.ShapeDtypeStruct((ROWS, D), bf16), i...  61.7 us

profile of v2, /device:TPU:1, one launch (start us, length us, event | category | flops | bytes accessed | tf_op | source)
XLA Modules:
  0.0 62.7 jit_solution(8254607499464723045)
XLA Ops:
  0.0 61.7 %layer.1 = bf16[128,4096]{1,0:T(8,128)(2,1)S(1)} custom-call(f32[16]{0:T(128)} %lam_hbm.1, bf16[128,2048]{1,0:T(8,128)(2,1)} %bitcast.7, bf16[128,512]{1,0:T(8,128)(2,1)} %bitcast.8, bf16[128,512]{1,0:T(8,128)(2,1)} %bitcast.9, f32[1,128]{1,0:T(1,128)} %bitcast.11, f32[2,128,128]{2,1,0:T(8,128)} %constant.4.clone.inner_hbm, ...), custom_call_target="tpu_custom_call" | custom-call | tf_op jit(solution)/shard_map/layer/pallas_call | solution.py:523
  61.7 1.0 %copy.10 = bf16[1,128,4096]{2,1,0:T(8,128)(2,1)} copy(bf16[1,128,4096]{2,1,0:T(8,128)(2,1)S(1)} %bitcast.6) | data formatting | bytes 2097152

commit v3 on v2

--- a/solution.py
+++ b/solution.py
@@ -23,6 +23,19 @@
 MESH = pl.DeviceIdType.MESH
 
 COLOURS = ((0, 1024), (1024, 512), (1536, 512))
+
+ORDER = (
+    "kvy0s", "x300s", "z1s", "kvzs", "y1s", "x1s", "x20s", "rotq", "qs", "kvy0f", "x300f", "kvz3w", "kvy3s",
+    "kvz1w", "kvy1s", "z1f", "x20f", "x301s", "x303s", "y1f", "kvz2w", "kvy2s", "x1f", "x310s", "x330s",
+    "z1e", "z2s", "x21s", "z30s", "x23s", "kvy3f", "x301f", "kvy1f", "x20e", "x303f", "x302s", "y1e", "y2s",
+    "y30s", "kvy2f", "x310f", "x1e", "x320s", "x22s", "x330f", "z2f", "z33s", "z31s", "x21f", "x311s",
+    "x313s", "z30f", "x302f", "x23f", "x333s", "x331s", "x320f", "y2f", "y33s", "y31s", "x311f", "y30f",
+    "z33f", "x313f", "kvall", "at00", "at01", "x333f", "x22f", "x321s", "x323s", "at02", "z2e", "z32s",
+    "at10", "x21e", "x312s", "x23e", "x332s", "x331f", "at11", "at12", "y2e", "y32s", "at20", "at21", "x321f",
+    "at22", "x323f", "at30", "at31", "x312f", "at32", "x332f", "y30e", "z31f", "y31f", "y33f", "z33e", "o1w",
+    "x22e", "x322s", "z30e", "z32f", "y32f", "o3w", "o2w", "y31e", "z31e", "x322f", "acts", "py0", "pxz3",
+    "pxz1", "y33e", "py3", "py1", "pxz0", "sw0", "z32e", "y32e", "py2", "pxz2", "sw1", "m0", "m1",
+)
 
 
 def rotation_tables():
@@ -207,64 +220,35 @@
         arrived(4 * x3[0, b].bytes, x3[0, b].fin, f"finx{b}")
 
     c_w.wait()
-    for ring in (x1, x2[0], x3[0, 0], y1, z1):
-        ring.start()
-    for o in (1, 3, 2):
-        kvz_start(o)
-    kvy_start(0)
-
-    with jax.named_scope("rotq"):
-        c_q.wait()
-        for g in range(KV_HEADS):
-            for h in range(GROUP):
-                a = (g * GROUP + h) * 128
-                qst[g, :, h * 128:(h + 1) * 128] = rotate(q_in[:, a:a + 128])
-    qin[me["z"]] = qst[me["z"]]
-    x1.forward()
-    for ring in (x3[3, 0], x3[1, 0]):
-        ring.start()
-    kvz_wait(3)
-    kvy_start(3)
-    kvz_wait(1)
-    kvy_start(1)
-    for o in (1, 3, 2):
-        pos = shift("z", o)
-        send(qst.at[pos["z"]], qin.at[me["z"]], q_r.at[o - 1], at(pos))
-    x2[0].forward()
-    for ring in (x3[0, 3], x3[0, 1]):
-        ring.start()
-    y1.forward()
-    z1.forward()
-    kvy_forward(0)
-    for ring in (x2[3], x2[1]):
-        ring.start()
-    x3[0, 0].forward()
-    x1.finish()
-    x3[2, 0].start()
-    kvz_wait(2)
-    kvy_start(2)
-    x2[2].start()
-    y1.finish()
-    z1.finish()
-    y2.start()
-    z3[0].start()
-    kvy_forward(3)
-    kvy_forward(1)
-    x2[0].finish()
-    x3[0, 2].start()
-    x3[3, 0].forward()
-    x3[1, 0].forward()
-    for a in (3, 1):
-        x2[a].forward()
-        x3[a, 3].start()
-        x3[a, 1].start()
-    kvy_forward(2)
-    pacc[...] = jnp.zeros_like(pacc)
-    z2.start()
-    y3[0].start()
-    x3[0, 3].forward()
-    x3[0, 1].forward()
-    arrived(4 * block_bytes, kvy_r.at[4], "kvyf")
+    tasks = {"kvzs": lambda: [kvz_start(o) for o in (1, 3, 2)]}
+    for a in steps:
+        tasks[f"kvz{a}w"] = functools.partial(kvz_wait, a)
+        tasks[f"kvy{a}s"] = functools.partial(kvy_start, a)
+        tasks[f"kvy{a}f"] = functools.partial(kvy_forward, a)
+    tasks["kvall"] = lambda: arrived(4 * block_bytes, kvy_r.at[4], "kvyf")
+    rings = {"x1": x1, "y1": y1, "z1": z1, "y2": y2, "z2": z2}
+    for a in steps:
+        rings.update({f"x2{a}": x2[a], f"y3{a}": y3[a], f"z3{a}": z3[a]})
+        rings.update({f"x3{a}{b}": x3[a, b] for b in steps})
+    for name, ring in rings.items():
+        tasks.update({name + "s": ring.start, name + "f": ring.forward, name + "e": ring.finish})
+
+    def rotate_queries():
+        with jax.named_scope("rotq"):
+            c_q.wait()
+            for g in range(KV_HEADS):
+                for h in range(GROUP):
+                    a = (g * GROUP + h) * 128
+                    qst[g, :, h * 128:(h + 1) * 128] = rotate(q_in[:, a:a + 128])
+            qin[me["z"]] = qst[me["z"]]
+            pacc[...] = jnp.zeros_like(pacc)
+
+    def send_queries():
+        for o in (1, 3, 2):
+            pos = shift("z", o)
+            send(qst.at[pos["z"]], qin.at[me["z"]], q_r.at[o - 1], at(pos))
+
+    tasks.update({"rotq": rotate_queries, "qs": send_queries})
 
     scale = float(HEAD_DIM ** -0.5 * np.log2(np.e))
     c_lam.wait()
@@ -274,7 +258,12 @@
     lane = lax.broadcasted_iota(jnp.int32, (128, 128), 1)
     half_rows = GROUP * ROWS
 
-    def attend(i, after):
+    kept = {}
+
+    def fold(x, op):
+        return op(x.reshape(KT // 8, 8, x.shape[1]), 0)
+
+    def attend_scores(i):
         zq = lax.rem(me["z"] + 1 + i, 4)
         if i < 3:
             o = 3 - i
@@ -293,17 +282,11 @@
             keys = jnp.concatenate([kv[4 * t + b, 0] for b in range(4)], 0)
             return lax.dot_general(keys, q2[...], (((1,), (1,)), ((), ())), preferred_element_type=f32)
 
-        def fold(x, op):
-            r = x.reshape(KT // 8, 8, x.shape[1])
-            return op(r, 0)
-
         def pass1(t, top):
             s = scores(t)
             sbuf[t] = s
             return jnp.maximum(top, fold(s, jnp.max))
 
-        scope = jax.named_scope(f"pass1_{i}")
-        scope.__enter__()
         top = lax.fori_loop(0, last, pass1, jnp.full((8, 2 * half_rows), -1e30, f32))
         s = scores(last)
         key_at = lax.broadcasted_iota(jnp.int32, (KT, 2 * half_rows), 0) + last * KT
@@ -312,18 +295,23 @@
         sbuf[last] = s
         top = jnp.maximum(top, fold(s, jnp.max))
         top = jnp.max(top, 0, keepdims=True)
-        scope.__exit__(None, None, None)
-        after[0]()
+        kept["top"] = top
+
+    def attend_exp(i):
+        last = lax.rem(me["z"] + 1 + i, 4)
+        top = kept["top"]
 
         def pass2(t, total):
             p = jnp.exp2((sbuf[t] - top) * scale)
             sbuf[t] = p
             return total + fold(p, jnp.sum)
 
-        with jax.named_scope(f"pass2_{i}"):
-            total = lax.fori_loop(0, last + 1, pass2, jnp.zeros((8, 2 * half_rows), f32))
-        after[1]()
-        total = jnp.sum(total, 0, keepdims=True)
+        total = lax.fori_loop(0, last + 1, pass2, jnp.zeros((8, 2 * half_rows), f32))
+        kept["total"] = jnp.sum(total, 0, keepdims=True)
+
+    def attend_values(i):
+        zq = last = lax.rem(me["z"] + 1 + i, 4)
+        total = kept["total"]
         a0 = 1.0 / total[:, :half_rows]
         a1 = lam / total[:, half_rows:]
         acc[...] = jnp.zeros_like(acc)
@@ -334,16 +322,14 @@
             acc[...] += jnp.dot(vals, w, preferred_element_type=f32)
             return carry
 
-        with jax.named_scope(f"pass3_{i}"):
-            lax.fori_loop(0, last + 1, pass3, 0)
-        after[2]()
+        lax.fori_loop(0, last + 1, pass3, 0)
         hv = acc[...]
         inv = lax.rsqrt(jnp.mean(hv * hv, 0, keepdims=True) + NORM_EPS)
         hv = hv * inv
         for h in range(GROUP):
             piece = hv[:, h * 128:(h + 1) * 128].T
             hst[zq, :, h * 128:(h + 1) * 128] = (piece * gain_ref[...] * OUTPUT_SCALE).astype(bf16)
-        return zq
+        ship(i, zq)
 
     def ship(i, zq):
         if i < 3:
@@ -415,96 +401,33 @@
                 cols = pl.ds(pl.multiple_of((z * 4 + y) * 256, 256), 256)
                 out_ref[:, cols] = jnp.dot(both, spread, preferred_element_type=f32).astype(bf16)
 
-    def nothing():
-        pass
-
-    def h00():
-        x2[2].forward()
-        x3[2, 3].start()
-        x3[2, 1].start()
-
-    def h01():
-        for a in (3, 1):
-            x2[a].finish()
-            x3[a, 2].start()
-        x3[2, 0].forward()
-
-    def h10():
-        y2.forward()
-        y3[3].start()
-        y3[1].start()
-        x3[0, 2].forward()
-
-    def h11():
-        x2[2].finish()
-        x3[2, 2].start()
-        z2.forward()
-        z3[3].start()
-        z3[1].start()
-
-    def h12():
-        x3[3, 3].forward()
-
-    def h20():
-        x3[3, 1].forward()
-        z3[0].forward()
-
-    def h21():
-        y2.finish()
-        y3[2].start()
-
-    def h22():
-        z2.finish()
-        z3[2].start()
-        y3[0].forward()
-        x3[1, 3].forward()
-
-    def h30():
-        x3[1, 1].forward()
-        x3[2, 3].forward()
-
+    def scoped(name, fn, *args):
+        with jax.named_scope(name):
+            fn(*args)
+
+    def project_xz_task(b):
+        x3_finish(b)
+        project_xz(b)
+
+    for i in range(4):
+        for n, fn in enumerate((attend_scores, attend_exp, attend_values)):
+            tasks[f"at{i}{n}"] = functools.partial(scoped, f"at{i}{n}", fn, i)
+    for o in (1, 2, 3):
+        tasks[f"o{o}w"] = functools.partial(acts_in, o)
+    tasks["acts"] = lambda: arrived(4 * size(acts.at[0, 0]), af_r.at[0], "acts")
+    for b in steps:
+        tasks[f"pxz{b}"] = functools.partial(project_xz_task, b)
+        tasks[f"py{b}"] = functools.partial(project_y, b)
+    tasks["sw0"] = functools.partial(swap_tiles, early, 0)
+    tasks["sw1"] = functools.partial(swap_tiles, late, 1)
+    tasks["m0"] = functools.partial(merge, early, 0)
+    tasks["m1"] = functools.partial(merge, late, 1)
     c_gain.wait()
-    hooks = ((h00, h01, nothing), (h10, h11, h12), (h20, h21, h22), (h30, nothing, nothing))
-    for i in range(4):
-        ship(i, attend(i, hooks[i]))
-    acts_in(1)
-    x3[2, 1].forward()
-    acts_in(2)
-    acts_in(3)
-    z3[3].forward()
-    y3[3].forward()
-    x3_finish(0)
-    z3[0].finish()
-    x3[3, 2].forward()
-    arrived(4 * size(acts.at[0, 0]), af_r.at[0], "acts")
-    project_xz(0)
-    z3[1].forward()
-    y3[1].forward()
-    x3[1, 2].forward()
-    y3[0].finish()
-    project_y(0)
-    x3[2, 2].forward()
-    x3_finish(3)
-    z3[3].finish()
-    project_xz(3)
-    z3[2].forward()
-    y3[2].forward()
-    y3[3].finish()
-    project_y(3)
-    x3_finish(1)
-    z3[1].finish()
-    project_xz(1)
-    y3[1].finish()
-    project_y(1)
-    swap_tiles(early, 0)
-    x3_finish(2)
-    z3[2].finish()
-    project_xz(2)
-    y3[2].finish()
-    project_y(2)
-    swap_tiles(late, 1)
-    merge(early, 0)
-    merge(late, 1)
+    left = [n for n in tasks if not (n.startswith("x3") and n.endswith("e"))]
+    left.remove("kvz0w")
+    assert sorted(left) == sorted(ORDER)
+    for name in ORDER:
+        tasks[name]()
     with jax.named_scope("drain"):
         for kind in (0, 1):
             view = amount(total_sent[kind])

time: 62.8 us -> 55.8 us (0.89)
  Pallas kernels: 61.7 us -> 54.7 us
    pallas_call x1, Pallas kernels: 61.7 us -> 54.7 us  [shards(): pl.pallas_call(kernel, out_shape=jax.ShapeDtypeStruct((ROWS, D), bf16), i...]
where the time goes in v3:
time: 55.8 us; the launch traced here: 55.7 us
  Pallas kernels  54.7 us (98%)
  local copies, waits for them, and re-layouts  0.97 us (2%)
    pallas_call x1, Pallas kernels, shards(): pl.pallas_call(kernel, out_shape=jax.ShapeDtypeStruct((ROWS, D), bf16), i...  54.7 us

profile of v3, /device:TPU:1, one launch (start us, length us, event | category | flops | bytes accessed | tf_op | source)
XLA Modules:
  0.0 55.7 jit_solution(13483758389455273971)
XLA Ops:
  0.0 54.7 %layer.1 = bf16[128,4096]{1,0:T(8,128)(2,1)S(1)} custom-call(f32[16]{0:T(128)} %lam_hbm.1, bf16[128,2048]{1,0:T(8,128)(2,1)} %bitcast.7, bf16[128,512]{1,0:T(8,128)(2,1)} %bitcast.8, bf16[128,512]{1,0:T(8,128)(2,1)} %bitcast.9, f32[1,128]{1,0:T(1,128)} %bitcast.11, f32[2,128,128]{2,1,0:T(8,128)} %constant.4.clone.inner_hbm, ...), custom_call_target="tpu_custom_call" | custom-call | tf_op jit(solution)/shard_map/layer/pallas_call | solution.py:446
  54.7 1.0 %copy.10 = bf16[1,128,4096]{2,1,0:T(8,128)(2,1)} copy(bf16[1,128,4096]{2,1,0:T(8,128)(2,1)S(1)} %bitcast.6) | data formatting | bytes 2097152

commit v4 on v3

--- a/solution.py
+++ b/solution.py
@@ -24,17 +24,19 @@
 
 COLOURS = ((0, 1024), (1024, 512), (1536, 512))
 
+DIRECT = (2,)
 ORDER = (
-    "kvy0s", "x300s", "z1s", "kvzs", "y1s", "x1s", "x20s", "rotq", "qs", "kvy0f", "x300f", "kvz3w", "kvy3s",
-    "kvz1w", "kvy1s", "z1f", "x20f", "x301s", "x303s", "y1f", "kvz2w", "kvy2s", "x1f", "x310s", "x330s",
-    "z1e", "z2s", "x21s", "z30s", "x23s", "kvy3f", "x301f", "kvy1f", "x20e", "x303f", "x302s", "y1e", "y2s",
-    "y30s", "kvy2f", "x310f", "x1e", "x320s", "x22s", "x330f", "z2f", "z33s", "z31s", "x21f", "x311s",
-    "x313s", "z30f", "x302f", "x23f", "x333s", "x331s", "x320f", "y2f", "y33s", "y31s", "x311f", "y30f",
-    "z33f", "x313f", "kvall", "at00", "at01", "x333f", "x22f", "x321s", "x323s", "at02", "z2e", "z32s",
-    "at10", "x21e", "x312s", "x23e", "x332s", "x331f", "at11", "at12", "y2e", "y32s", "at20", "at21", "x321f",
-    "at22", "x323f", "at30", "at31", "x312f", "at32", "x332f", "y30e", "z31f", "y31f", "y33f", "z33e", "o1w",
-    "x22e", "x322s", "z30e", "z32f", "y32f", "o3w", "o2w", "y31e", "z31e", "x322f", "acts", "py0", "pxz3",
-    "pxz1", "y33e", "py3", "py1", "pxz0", "sw0", "z32e", "y32e", "py2", "pxz2", "sw1", "m0", "m1",
+    "x20s", "z1s", "y1s", "x300s", "x1s", "rotk", "kvzs", "kvy0s", "rotq", "kvy0f", "qs", "z1f", "kvz1w",
+    "kvy1s", "kvz3w", "kvy3s", "x20f", "x301s", "y1f", "x303s", "x1f", "x310s", "x330s", "x300f", "kvz2w",
+    "kvy2s", "z1e", "z30s", "kvy1f", "z2s", "x21s", "x301f", "y1e", "y2s", "kvy3f", "x23s", "x303f", "x20e",
+    "x302s", "x310f", "x1e", "x320s", "x22s", "x330f", "z30f", "x302f", "z2f", "z31s", "z33s", "x21f", "y2f",
+    "y33s", "x313s", "x311s", "x320f", "kvall", "at00", "at01", "x23f", "x331s", "at02", "x22f", "x323s",
+    "x321s", "y30s", "at10", "z2e", "z32s", "x313f", "at11", "x311f", "x21e", "x312s", "at12", "y31s", "at20",
+    "x331f", "at21", "y2e", "y32s", "at22", "x323f", "x23e", "x332s", "at30", "x321f", "at31", "o1w", "at32",
+    "y30f", "x333s", "z30e", "z31f", "x302e", "z33f", "y33f", "x22e", "x322s", "x312f", "z32f", "y31f",
+    "x332f", "o3w", "o2w", "x333f", "z31e", "y32f", "acts", "pxz1", "z33e", "pxz0", "x312e", "x322f", "y30e",
+    "py0", "y33e", "py3", "z32e", "pz2", "pxz3", "y31e", "py1", "sw0", "x332e", "px0", "y32e", "py2", "sw1",
+    "x322e", "px2", "sw2", "m0", "m1", "m2",
 )
 
 
@@ -93,7 +95,7 @@
             ).wait_recv()
 
     barrier = pltpu.get_barrier_semaphore()
-    peers = [at(shift("z", o)) for o in (1, 2, 3)] + [at(shift("y", o)) for o in (1, 3)]
+    peers = [at(shift("z", o)) for o in (1, 2, 3)] + [at(shift("y", o)) for o in ((1, 2, 3) if DIRECT else (1, 3))]
     peers += [at(shift("x", o)) for o in (1, 3)] + [partner]
     for dev in peers:
         pl.semaphore_signal(barrier, inc=1, device_id=dev, device_id_type=MESH)
@@ -114,35 +116,38 @@
     for c in copies:
         c.start()
     c_k, c_in, c_out, c_v, c_w, c_q, c_gain, c_lam = copies
-    c_in.wait()
-    c_out.wait()
-
-    ci, si = inner_ref[0], inner_ref[1]
-    co, so = outer_ref[0:1, :], outer_ref[1:2, :]
-    cosine = co * ci - so * si
-    sine = so * ci + co * si
-    row = lax.broadcasted_iota(jnp.int32, (128, 128), 0)
-    col = lax.broadcasted_iota(jnp.int32, (128, 128), 1)
-    low = lax.rem(col, 64) < 32
-    swap = jnp.where(
-        low & (row == col + 32), -1.0, jnp.where(jnp.logical_not(low) & (row == col - 32), 1.0, 0.0)
-    ).astype(bf16)
-
-    def rotate(part):
-        turned = jnp.dot(part, swap, preferred_element_type=f32)
-        return (part.astype(f32) * cosine + turned * sine).astype(bf16)
-
-    with jax.named_scope("rotk"):
-        c_k.wait()
-        c_v.wait()
-        for g in range(KV_HEADS):
-            cols = slice(g * 128, (g + 1) * 128)
-            kvst[g, 0] = rotate(k_in[:, cols])
-            kvst[g, 1] = v_in[:, cols].astype(f32).T.astype(bf16)
-    kv[sp, 0] = kvst[me["z"], 0]
-    kv[sp, 1] = kvst[me["z"], 1]
     with jax.named_scope("barrier"):
         pl.semaphore_wait(barrier, len(peers))
+
+    def rotate(part):
+        turned = jnp.dot(part, kept["swap"], preferred_element_type=f32)
+        return (part.astype(f32) * kept["cosine"] + turned * kept["sine"]).astype(bf16)
+
+    kept = {}
+
+    def rotate_keys():
+        with jax.named_scope("rotk"):
+            row = lax.broadcasted_iota(jnp.int32, (128, 128), 0)
+            col = lax.broadcasted_iota(jnp.int32, (128, 128), 1)
+            low = lax.rem(col, 64) < 32
+            kept["swap"] = jnp.where(
+                low & (row == col + 32), -1.0, jnp.where(jnp.logical_not(low) & (row == col - 32), 1.0, 0.0)
+            ).astype(bf16)
+            c_v.wait()
+            for g in range(KV_HEADS):
+                kvst[g, 1] = v_in[:, g * 128:(g + 1) * 128].astype(f32).T.astype(bf16)
+            c_in.wait()
+            c_out.wait()
+            ci, si = inner_ref[0], inner_ref[1]
+            co, so = outer_ref[0:1, :], outer_ref[1:2, :]
+            kept["cosine"] = co * ci - so * si
+            kept["sine"] = so * ci + co * si
+            c_k.wait()
+            for g in range(KV_HEADS):
+                kvst[g, 0] = rotate(k_in[:, g * 128:(g + 1) * 128])
+            kv[sp, 0] = kvst[me["z"], 0]
+            kv[sp, 1] = kvst[me["z"], 1]
+            c_w.wait()
 
     steps = (0, 3, 1, 2)
     block_bytes = size(kv.at[0])
@@ -160,7 +165,9 @@
     def kvy_start(rel):
         view = kvst.at[me["z"]] if rel == 0 else kv.at[kv_block(rel, 0)]
         for off in (1, -1):
-            send(view, kv.at[kv_block(rel, 0)], kvy_r.at[rel], at(shift("y", off)))
+            send(view, kv.at[kv_block(rel, 0)], kvy_r.at[4 if rel in DIRECT else rel], at(shift("y", off)))
+        if rel in DIRECT:
+            send(view, kv.at[kv_block(rel, 0)], kvy_r.at[4], at(shift("y", 2)))
 
     def kvy_forward(rel):
         arrived(2 * block_bytes, kvy_r.at[rel], f"kvy_{rel}")
@@ -193,9 +200,11 @@
             return wbuf.at[sel["z"], sel["y"], sel["x"], rows, pl.ds(self.k0, self.kn)]
 
         def start(self):
-            view = self.view(0)
+            view = src = self.view(0)
+            if all(r == 0 for r in self.fixed.values()):
+                src = w_hbm.at[:, pl.ds(self.k0, self.kn)]
             for off in (1, -1):
-                send(view, view, self.full, at(shift(self.dim, off)), 1)
+                send(src, view, self.full, at(shift(self.dim, off)), 1)
 
         def forward(self):
             arrived(2 * self.bytes, self.full, "fwd" + self.name)
@@ -208,7 +217,7 @@
 
     x1 = Ring(0, "z", 0, y=0, x=0)
     x2 = {a: Ring(0, "y", 1 + a, z=a, x=0) for a in steps}
-    x3 = {(a, b): Ring(0, "x", 5 + b, z=a, y=b) for b in steps for a in steps}
+    x3 = {(a, b): Ring(0, "x", 21 + a if b == 2 else 5 + b, z=a, y=b) for b in steps for a in steps}
     y1 = Ring(1, "x", 9, z=0, y=0)
     y2 = Ring(1, "z", 10, x=None, y=0)
     y3 = {a: Ring(1, "y", 11 + a, x=None, z=a) for a in steps}
@@ -219,13 +228,13 @@
     def x3_finish(b):
         arrived(4 * x3[0, b].bytes, x3[0, b].fin, f"finx{b}")
 
-    c_w.wait()
     tasks = {"kvzs": lambda: [kvz_start(o) for o in (1, 3, 2)]}
     for a in steps:
         tasks[f"kvz{a}w"] = functools.partial(kvz_wait, a)
         tasks[f"kvy{a}s"] = functools.partial(kvy_start, a)
-        tasks[f"kvy{a}f"] = functools.partial(kvy_forward, a)
-    tasks["kvall"] = lambda: arrived(4 * block_bytes, kvy_r.at[4], "kvyf")
+        if a not in DIRECT:
+            tasks[f"kvy{a}f"] = functools.partial(kvy_forward, a)
+    tasks["kvall"] = lambda: arrived((4 + 2 * len(DIRECT)) * block_bytes, kvy_r.at[4], "kvyf")
     rings = {"x1": x1, "y1": y1, "z1": z1, "y2": y2, "z2": z2}
     for a in steps:
         rings.update({f"x2{a}": x2[a], f"y3{a}": y3[a], f"z3{a}": z3[a]})
@@ -248,7 +257,7 @@
             pos = shift("z", o)
             send(qst.at[pos["z"]], qin.at[me["z"]], q_r.at[o - 1], at(pos))
 
-    tasks.update({"rotq": rotate_queries, "qs": send_queries})
+    tasks.update({"rotk": rotate_keys, "rotq": rotate_queries, "qs": send_queries})
 
     scale = float(HEAD_DIM ** -0.5 * np.log2(np.e))
     c_lam.wait()
@@ -257,8 +266,6 @@
     )
     lane = lax.broadcasted_iota(jnp.int32, (128, 128), 1)
     half_rows = GROUP * ROWS
-
-    kept = {}
 
     def fold(x, op):
         return op(x.reshape(KT // 8, 8, x.shape[1]), 0)
@@ -364,6 +371,22 @@
             for z in range(4):
                 pacc[z, yb] += part[:, z * 128:(z + 1) * 128]
 
+    def project_x(places):
+        with jax.named_scope(f"proj_x{places[0]}"):
+            spots = [tile_of(a, 2) for a in places]
+            cat = jnp.concatenate([wbuf[z, y, :, :, 0:1024].reshape(128, 1024) for z, y in spots], 0)
+            part = multiply((0, 1), cat)
+            for n, (z, y) in enumerate(spots):
+                pacc[z, y] += part[:, n * 128:(n + 1) * 128]
+
+    def project_z(b):
+        with jax.named_scope(f"proj_z{b}"):
+            yb = lax.rem(me["y"] + b, 4)
+            cat = jnp.concatenate([wbuf[z, yb, :, :, 1536:2048].reshape(128, 512) for z in range(4)], 0)
+            part = multiply((3,), cat)
+            for z in range(4):
+                pacc[z, yb] += part[:, z * 128:(z + 1) * 128]
+
     def project_y(a):
         with jax.named_scope(f"proj_y{a}"):
             za = lax.rem(me["z"] + a, 4)
@@ -372,7 +395,7 @@
                 pacc[za, y] += part[:, y * 128:(y + 1) * 128]
 
     early = [(a, b) for a in (0, 3, 1) for b in (0, 3, 1)]
-    late = [(2, b) for b in (0, 3, 1)] + [(a, 2) for a in steps]
+    late = [(2, b) for b in (0, 3, 1)] + [(a, 2) for a in (0, 3, 1)]
 
     def tile_of(a, b):
         return lax.rem(me["z"] + a, 4), lax.rem(me["y"] + b, 4)
@@ -418,12 +441,15 @@
     for b in steps:
         tasks[f"pxz{b}"] = functools.partial(project_xz_task, b)
         tasks[f"py{b}"] = functools.partial(project_y, b)
-    tasks["sw0"] = functools.partial(swap_tiles, early, 0)
-    tasks["sw1"] = functools.partial(swap_tiles, late, 1)
-    tasks["m0"] = functools.partial(merge, early, 0)
-    tasks["m1"] = functools.partial(merge, late, 1)
+    del tasks["pxz2"]
+    tasks["px0"] = functools.partial(project_x, (0, 3, 1))
+    tasks["px2"] = functools.partial(project_x, (2,))
+    tasks["pz2"] = functools.partial(project_z, 2)
+    for n, tiles in enumerate((early, late, [(2, 2)])):
+        tasks[f"sw{n}"] = functools.partial(swap_tiles, tiles, n)
+        tasks[f"m{n}"] = functools.partial(merge, tiles, n)
     c_gain.wait()
-    left = [n for n in tasks if not (n.startswith("x3") and n.endswith("e"))]
+    left = [n for n in tasks if not (n.startswith("x3") and n.endswith("e") and n[3] != "2")]
     left.remove("kvz0w")
     assert sorted(left) == sorted(ORDER)
     for name in ORDER:
@@ -470,7 +496,7 @@
             pltpu.VMEM((4, 4, 128, 128), bf16),
             pltpu.VMEM((4, 4, 128, 128), bf16),
             pltpu.VMEM((4, 4, 128, 128), bf16),
-            dma(8), dma(2), dma(3), dma(5), dma(3), dma(33), dma(21), dma(3), dma(1), dma(2),
+            dma(8), dma(2), dma(3), dma(5), dma(3), dma(33), dma(25), dma(3), dma(1), dma(3),
         ],
         compiler_params=pltpu.CompilerParams(
             collective_id=0, has_side_effects=True, vmem_limit_bytes=50_000_000

time: 55.8 us -> 54.5 us (0.977)
  Pallas kernels: 54.7 us -> 53.4 us
    pallas_call x1, Pallas kernels: 54.7 us -> 53.4 us  [shards(): pl.pallas_call(kernel, out_shape=jax.ShapeDtypeStruct((ROWS, D), bf16), i...]
where the time goes in v4:
time: 54.5 us; the launch traced here: 54.4 us
  Pallas kernels  53.4 us (98%)
  local copies, waits for them, and re-layouts  0.97 us (2%)
    pallas_call x1, Pallas kernels, shards(): pl.pallas_call(kernel, out_shape=jax.ShapeDtypeStruct((ROWS, D), bf16), i...  53.4 us

profile of v4, /device:TPU:1, one launch (start us, length us, event | category | flops | bytes accessed | tf_op | source)
XLA Modules:
  0.0 54.4 jit_solution(9363269760048874038)
XLA Ops:
  0.0 53.4 %layer.1 = bf16[128,4096]{1,0:T(8,128)(2,1)S(1)} custom-call(f32[16]{0:T(128)} %lam_hbm.1, bf16[128,2048]{1,0:T(8,128)(2,1)} %bitcast.7, bf16[128,512]{1,0:T(8,128)(2,1)} %bitcast.8, bf16[128,512]{1,0:T(8,128)(2,1)} %bitcast.9, f32[1,128]{1,0:T(1,128)} %bitcast.11, f32[2,128,128]{2,1,0:T(8,128)} %constant.4.clone.inner_hbm, ...), custom_call_target="tpu_custom_call" | custom-call | tf_op jit(solution)/shard_map/layer/pallas_call | solution.py:472
  53.4 1.0 %copy.10 = bf16[1,128,4096]{2,1,0:T(8,128)(2,1)} copy(bf16[1,128,4096]{2,1,0:T(8,128)(2,1)S(1)} %bitcast.6) | data formatting | bytes 2097152

commit v5 on v4

--- a/solution.py
+++ b/solution.py
@@ -24,19 +24,19 @@
 
 COLOURS = ((0, 1024), (1024, 512), (1536, 512))
 
-DIRECT = (2,)
+DIRECT = ()
 ORDER = (
-    "x20s", "z1s", "y1s", "x300s", "x1s", "rotk", "kvzs", "kvy0s", "rotq", "kvy0f", "qs", "z1f", "kvz1w",
-    "kvy1s", "kvz3w", "kvy3s", "x20f", "x301s", "y1f", "x303s", "x1f", "x310s", "x330s", "x300f", "kvz2w",
-    "kvy2s", "z1e", "z30s", "kvy1f", "z2s", "x21s", "x301f", "y1e", "y2s", "kvy3f", "x23s", "x303f", "x20e",
-    "x302s", "x310f", "x1e", "x320s", "x22s", "x330f", "z30f", "x302f", "z2f", "z31s", "z33s", "x21f", "y2f",
-    "y33s", "x313s", "x311s", "x320f", "kvall", "at00", "at01", "x23f", "x331s", "at02", "x22f", "x323s",
-    "x321s", "y30s", "at10", "z2e", "z32s", "x313f", "at11", "x311f", "x21e", "x312s", "at12", "y31s", "at20",
-    "x331f", "at21", "y2e", "y32s", "at22", "x323f", "x23e", "x332s", "at30", "x321f", "at31", "o1w", "at32",
-    "y30f", "x333s", "z30e", "z31f", "x302e", "z33f", "y33f", "x22e", "x322s", "x312f", "z32f", "y31f",
-    "x332f", "o3w", "o2w", "x333f", "z31e", "y32f", "acts", "pxz1", "z33e", "pxz0", "x312e", "x322f", "y30e",
-    "py0", "y33e", "py3", "z32e", "pz2", "pxz3", "y31e", "py1", "sw0", "x332e", "px0", "y32e", "py2", "sw1",
-    "x322e", "px2", "sw2", "m0", "m1", "m2",
+    "x20s", "x1s", "z1s", "y1s", "x300s", "rotk", "kvzs", "kvy0s", "rotq", "kvy0f", "kvz3w", "kvy3s", "qs",
+    "kvz1w", "z1f", "kvy1s", "x20f", "x301s", "x1f", "x310s", "x303s", "y1f", "x330s", "kvz2w", "kvy2s",
+    "x300f", "z1e", "z30s", "kvy3f", "x301f", "kvy1f", "x23s", "x310f", "x20e", "x302s", "x303f", "y1e",
+    "y2s", "kvy2f", "z2s", "x21s", "x1e", "x22s", "x320s", "x330f", "x23f", "x331s", "x333s", "kvall", "at00",
+    "z30f", "x302f", "at01", "at02", "y2f", "y33s", "z2f", "z33s", "at10", "x21f", "x313s", "x311s", "at11",
+    "at12", "x331f", "x22f", "x323s", "y31s", "x321s", "z31s", "z30e", "at20", "x23e", "x332s", "x333f",
+    "at21", "at22", "x313f", "y30s", "o1w", "at30", "y2e", "y32s", "at31", "at32", "x22e", "x322s", "y33f",
+    "z2e", "z32s", "x21e", "x311f", "x302e", "x320f", "x312s", "x323f", "z33f", "x321f", "y31f", "x332f",
+    "o2w", "y30f", "x322f", "z31f", "o3w", "acts", "pxz0", "y32f", "x312f", "z32f", "y33e", "py3", "z33e",
+    "pxz3", "x332e", "y31e", "py1", "x322e", "px2", "z31e", "pxz1", "y30e", "py0", "sw0", "x312e", "px0",
+    "z32e", "pz2", "sw1", "y32e", "py2", "sw2", "m0", "m1", "m2",
 )
 
 
@@ -260,11 +260,6 @@
     tasks.update({"rotk": rotate_keys, "rotq": rotate_queries, "qs": send_queries})
 
     scale = float(HEAD_DIM ** -0.5 * np.log2(np.e))
-    c_lam.wait()
-    lam = jnp.concatenate(
-        [jnp.full((1, 128), lam_ref[me["z"] * GROUP + h], f32) for h in range(GROUP)], 1
-    )
-    lane = lax.broadcasted_iota(jnp.int32, (128, 128), 1)
     half_rows = GROUP * ROWS
 
     def fold(x, op):
@@ -275,6 +270,7 @@
         if i < 3:
             o = 3 - i
             arrived(size(qin.at[0]), q_r.at[o - 1], f"q_{i}")
+        lane = lax.broadcasted_iota(jnp.int32, (128, 128), 1)
         for m in range(2):
             keep = (lane < 64) if m == 0 else (lane >= 64)
             for h in range(GROUP):
@@ -319,6 +315,12 @@
     def attend_values(i):
         zq = last = lax.rem(me["z"] + 1 + i, 4)
         total = kept["total"]
+        if i == 0:
+            c_lam.wait()
+            c_gain.wait()
+        lam = jnp.concatenate(
+            [jnp.full((1, 128), lam_ref[me["z"] * GROUP + h], f32) for h in range(GROUP)], 1
+        )
         a0 = 1.0 / total[:, :half_rows]
         a1 = lam / total[:, half_rows:]
         acc[...] = jnp.zeros_like(acc)
@@ -395,7 +397,7 @@
                 pacc[za, y] += part[:, y * 128:(y + 1) * 128]
 
     early = [(a, b) for a in (0, 3, 1) for b in (0, 3, 1)]
-    late = [(2, b) for b in (0, 3, 1)] + [(a, 2) for a in (0, 3, 1)]
+    late = [(a, 2) for a in (0, 3, 1)]
 
     def tile_of(a, b):
         return lax.rem(me["z"] + a, 4), lax.rem(me["y"] + b, 4)
@@ -409,20 +411,23 @@
             send(opart.at[z, y], oin.at[z, y], oo_r.at[n], partner)
             oown[z, y] = pacc[z, y, :ROWS].astype(bf16)
 
-    erow = lax.broadcasted_iota(jnp.int32, (256, 256), 0)
-    ecol = lax.broadcasted_iota(jnp.int32, (256, 256), 1)
-    mine = jnp.where(erow < 128, core, 1 - core)
-    er = lax.rem(erow, 128)
-    spread = jnp.where(ecol == (er // 32) * 64 + mine * 32 + lax.rem(er, 32), 1.0, 0.0).astype(bf16)
+    def spread():
+        erow = lax.broadcasted_iota(jnp.int32, (256, 256), 0)
+        ecol = lax.broadcasted_iota(jnp.int32, (256, 256), 1)
+        mine = jnp.where(erow < 128, core, 1 - core)
+        er = lax.rem(erow, 128)
+        return jnp.where(ecol == (er // 32) * 64 + mine * 32 + lax.rem(er, 32), 1.0, 0.0).astype(bf16)
 
     def merge(tiles, n):
         arrived(len(tiles) * size(oin.at[0, 0]), oo_r.at[n], f"swap_{n}")
         with jax.named_scope(f"merge_{n}"):
+            if n == 0:
+                kept["spread"] = spread()
             for a, b in tiles:
                 z, y = tile_of(a, b)
                 both = jnp.concatenate([oown[z, y], oin[z, y]], 1)
                 cols = pl.ds(pl.multiple_of((z * 4 + y) * 256, 256), 256)
-                out_ref[:, cols] = jnp.dot(both, spread, preferred_element_type=f32).astype(bf16)
+                out_ref[:, cols] = jnp.dot(both, kept["spread"], preferred_element_type=f32).astype(bf16)
 
     def scoped(name, fn, *args):
         with jax.named_scope(name):
@@ -445,10 +450,9 @@
     tasks["px0"] = functools.partial(project_x, (0, 3, 1))
     tasks["px2"] = functools.partial(project_x, (2,))
     tasks["pz2"] = functools.partial(project_z, 2)
-    for n, tiles in enumerate((early, late, [(2, 2)])):
+    for n, tiles in enumerate((early, late, [(2, b) for b in steps])):
         tasks[f"sw{n}"] = functools.partial(swap_tiles, tiles, n)
         tasks[f"m{n}"] = functools.partial(merge, tiles, n)
-    c_gain.wait()
     left = [n for n in tasks if not (n.startswith("x3") and n.endswith("e") and n[3] != "2")]
     left.remove("kvz0w")
     assert sorted(left) == sorted(ORDER)

time: 54.5 us -> 53.5 us (0.982)
  Pallas kernels: 53.4 us -> 52.4 us
    pallas_call x1, Pallas kernels: 53.4 us -> 52.4 us  [shards(): pl.pallas_call(kernel, out_shape=jax.ShapeDtypeStruct((ROWS, D), bf16), i...]
where the time goes in v5:
time: 53.5 us; the launch traced here: 53.4 us
  Pallas kernels  52.4 us (98%)
  local copies, waits for them, and re-layouts  0.97 us (2%)
    pallas_call x1, Pallas kernels, shards(): pl.pallas_call(kernel, out_shape=jax.ShapeDtypeStruct((ROWS, D), bf16), i...  52.4 us

profile of v5, /device:TPU:1, one launch (start us, length us, event | category | flops | bytes accessed | tf_op | source)
XLA Modules:
  0.0 53.4 jit_solution(2187138646537672189)
XLA Ops:
  0.0 52.4 %layer.1 = bf16[128,4096]{1,0:T(8,128)(2,1)S(1)} custom-call(f32[16]{0:T(128)} %lam_hbm.1, bf16[128,2048]{1,0:T(8,128)(2,1)} %bitcast.7, bf16[128,512]{1,0:T(8,128)(2,1)} %bitcast.8, bf16[128,512]{1,0:T(8,128)(2,1)} %bitcast.9, f32[1,128]{1,0:T(1,128)} %bitcast.11, f32[2,128,128]{2,1,0:T(8,128)} %constant.4.clone.inner_hbm, ...), custom_call_target="tpu_custom_call" | custom-call | tf_op jit(solution)/shard_map/layer/pallas_call | solution.py:476
  52.5 1.0 %copy.10 = bf16[1,128,4096]{2,1,0:T(8,128)(2,1)} copy(bf16[1,128,4096]{2,1,0:T(8,128)(2,1)S(1)} %bitcast.6) | data formatting | bytes 2097152

commit v6 on v5

--- a/solution.py
+++ b/solution.py
@@ -34,9 +34,9 @@
     "at12", "x331f", "x22f", "x323s", "y31s", "x321s", "z31s", "z30e", "at20", "x23e", "x332s", "x333f",
     "at21", "at22", "x313f", "y30s", "o1w", "at30", "y2e", "y32s", "at31", "at32", "x22e", "x322s", "y33f",
     "z2e", "z32s", "x21e", "x311f", "x302e", "x320f", "x312s", "x323f", "z33f", "x321f", "y31f", "x332f",
-    "o2w", "y30f", "x322f", "z31f", "o3w", "acts", "pxz0", "y32f", "x312f", "z32f", "y33e", "py3", "z33e",
-    "pxz3", "x332e", "y31e", "py1", "x322e", "px2", "z31e", "pxz1", "y30e", "py0", "sw0", "x312e", "px0",
-    "z32e", "pz2", "sw1", "y32e", "py2", "sw2", "m0", "m1", "m2",
+    "o2w", "y30f", "x322f", "z31f", "o3w", "acts", "y32f", "x312f", "z32f", "y33e", "z33e", "pxz0", "x332e",
+    "y31e", "x322e", "z31e", "pxz1", "y30e", "py0", "sw0", "x312e", "px0", "z32e", "pz2", "sw1", "y32e",
+    "py2", "sw2", "m0", "m1", "m2",
 )
 
 
@@ -363,15 +363,15 @@
             total = part if total is None else total + part
         return total
 
-    def project_xz(b):
-        with jax.named_scope(f"proj_xz{b}"):
-            yb = lax.rem(me["y"] + b, 4)
+    def project_xz(places):
+        with jax.named_scope(f"proj_xz{places[0]}"):
+            spots = [(z, lax.rem(me["y"] + b, 4)) for b in places for z in range(4)]
             cat = lambda lo, hi: jnp.concatenate(
-                [wbuf[z, yb, :, :, lo:hi].reshape(128, hi - lo) for z in range(4)], 0
+                [wbuf[z, y, :, :, lo:hi].reshape(128, hi - lo) for z, y in spots], 0
             )
             part = multiply((0, 1), cat(0, 1024)) + multiply((3,), cat(1536, 2048))
-            for z in range(4):
-                pacc[z, yb] += part[:, z * 128:(z + 1) * 128]
+            for n, (z, y) in enumerate(spots):
+                pacc[z, y] += part[:, n * 128:(n + 1) * 128]
 
     def project_x(places):
         with jax.named_scope(f"proj_x{places[0]}"):
@@ -389,12 +389,14 @@
             for z in range(4):
                 pacc[z, yb] += part[:, z * 128:(z + 1) * 128]
 
-    def project_y(a):
-        with jax.named_scope(f"proj_y{a}"):
-            za = lax.rem(me["z"] + a, 4)
-            part = multiply((2,), wbuf[za, :, :, :, 1024:1536].reshape(512, 512))
-            for y in range(4):
-                pacc[za, y] += part[:, y * 128:(y + 1) * 128]
+    def project_y(places):
+        with jax.named_scope(f"proj_y{places[0]}"):
+            spots = [lax.rem(me["z"] + a, 4) for a in places]
+            cat = jnp.concatenate([wbuf[z, :, :, :, 1024:1536].reshape(512, 512) for z in spots], 0)
+            part = multiply((2,), cat)
+            for n, z in enumerate(spots):
+                for y in range(4):
+                    pacc[z, y] += part[:, (n * 4 + y) * 128:(n * 4 + y + 1) * 128]
 
     early = [(a, b) for a in (0, 3, 1) for b in (0, 3, 1)]
     late = [(a, 2) for a in (0, 3, 1)]
@@ -433,9 +435,10 @@
         with jax.named_scope(name):
             fn(*args)
 
-    def project_xz_task(b):
-        x3_finish(b)
-        project_xz(b)
+    def project_xz_task(places):
+        for b in places:
+            x3_finish(b)
+        project_xz(places)
 
     for i in range(4):
         for n, fn in enumerate((attend_scores, attend_exp, attend_values)):
@@ -443,12 +446,11 @@
     for o in (1, 2, 3):
         tasks[f"o{o}w"] = functools.partial(acts_in, o)
     tasks["acts"] = lambda: arrived(4 * size(acts.at[0, 0]), af_r.at[0], "acts")
-    for b in steps:
-        tasks[f"pxz{b}"] = functools.partial(project_xz_task, b)
-        tasks[f"py{b}"] = functools.partial(project_y, b)
-    del tasks["pxz2"]
-    tasks["px0"] = functools.partial(project_x, (0, 3, 1))
-    tasks["px2"] = functools.partial(project_x, (2,))
+    tasks["pxz0"] = functools.partial(project_xz_task, (0, 3))
+    tasks["pxz1"] = functools.partial(project_xz_task, (1,))
+    tasks["py0"] = functools.partial(project_y, (0, 3, 1))
+    tasks["py2"] = functools.partial(project_y, (2,))
+    tasks["px0"] = functools.partial(project_x, steps)
     tasks["pz2"] = functools.partial(project_z, 2)
     for n, tiles in enumerate((early, late, [(2, b) for b in steps])):
         tasks[f"sw{n}"] = functools.partial(swap_tiles, tiles, n)

time: 53.5 us -> 53.4 us (level)
  no operation moved by 1% of the time
where the time goes in v6:
time: 53.4 us; the launch traced here: 53.3 us
  Pallas kernels  52.3 us (98%)
  local copies, waits for them, and re-layouts  0.97 us (2%)
    pallas_call x1, Pallas kernels, shards(): pl.pallas_call(kernel, out_shape=jax.ShapeDtypeStruct((ROWS, D), bf16), i...  52.3 us

profile of v6, /device:TPU:1, one launch (start us, length us, event | category | flops | bytes accessed | tf_op | source)
XLA Modules:
  0.0 53.3 jit_solution(4861056687453680859)
XLA Ops:
  0.0 52.3 %layer.1 = bf16[128,4096]{1,0:T(8,128)(2,1)S(1)} custom-call(f32[16]{0:T(128)} %lam_hbm.1, bf16[128,2048]{1,0:T(8,128)(2,1)} %bitcast.7, bf16[128,512]{1,0:T(8,128)(2,1)} %bitcast.8, bf16[128,512]{1,0:T(8,128)(2,1)} %bitcast.9, f32[1,128]{1,0:T(1,128)} %bitcast.11, f32[2,128,128]{2,1,0:T(8,128)} %constant.4.clone.inner_hbm, ...), custom_call_target="tpu_custom_call" | custom-call | tf_op jit(solution)/shard_map/layer/pallas_call | solution.py:478
  52.3 1.0 %copy.10 = bf16[1,128,4096]{2,1,0:T(8,128)(2,1)} copy(bf16[1,128,4096]{2,1,0:T(8,128)(2,1)S(1)} %bitcast.6) | data formatting | bytes 2097152
